TPU v7x, 512 devices: a whole 4x8x8 slice. The times are simulated.
512 devices in a mesh: ep: 32 (over z, x), tp: 16 (over y, core).
Axes of the slice: x: 4, y: 8, z: 8, core: 2. Of those that a mesh axis runs over, the one named last changes fastest.
Arguments:
- query_latent: bfloat16 [8192, 768], P('ep'), may hold values from -600 to 600
- shared_latent: bfloat16 [8192, 512], P('ep'), may hold values from -600 to 600
- rotary_key: bfloat16 [8192, 64], P('ep'), may hold values from -2500 to 2500
- query_gain: float32 [768], replicated, may hold values from 0.1 to 1.9
- shared_gain: float32 [512], replicated, may hold values from 0.1 to 1.9
- query_plain_weight: bfloat16 [768, 2048], P(None, 'tp'), may hold values from -0.21875 to 0.21875
- query_turn_weight: bfloat16 [768, 1024], P(None, 'tp'), may hold values from -0.21875 to 0.21875
- key_weight: bfloat16 [512, 2048], P(None, 'tp'), may hold values from -0.25 to 0.25
- value_weight: bfloat16 [512, 2048], P(None, 'tp'), may hold values from -0.25 to 0.25
- mixer_out_weight: bfloat16 [2048, 2048], P('tp'), may hold values from -1 to 1
- expert_input: bfloat16 [4096, 2048], P('ep'), may hold values from -600 to 600
- expert_gain: float32 [2048], replicated, may hold values from 0.1 to 1.9
- routing: int32 [4096, 4], P('ep'), may hold values from 0 to 31, all different within a row; in each aligned block of 128 rows (0 to 127, 128 to 255, ...) at most 21 rows name the same one
- routing_weight: float32 [4096, 4], P('ep'), may hold values from 0.05 to 1
- gate_weight: bfloat16 [32, 2048, 2048], P('ep', None, 'tp'), may hold values from -0.375 to 0.375
- up_weight: bfloat16 [32, 2048, 2048], P('ep', None, 'tp'), may hold values from -0.375 to 0.375
- down_weight: bfloat16 [32, 2048, 2048], P('ep', 'tp'), may hold values from -0.01953125 to 0.01953125
Outputs:
- mixer_output: bfloat16 [8192, 2048], P('ep')
- expert_output: bfloat16 [4096, 2048], P('ep')
Inputs may be any that keep to these rules, and one draw needn't show every extreme that they name: `routing`: each row names 4 different experts. In each aligned block of 128 rows (the rows of one index of ep) no expert is named by more than 21 rows, and in some block some expert is named by exactly 21.
All inputs are finite; a program needn't handle non-finite values.
Results may differ from a plain program's by a relative error of at most 0.019.
Values may be sent and summed in bfloat16 or wider, within the bound.
A program may use at most 128 MiB of HBM per device.

v0:
```python
import jax
import jax.numpy as jnp
from jax import lax
from jax.sharding import Mesh
from jax.sharding import PartitionSpec as P

NOPE = 128
ROPE = 64
VDIM = 128
TP = ("tp_0", "tp_1")


EPSILON = 1e-06
CLAMP_LIMIT = 7.0
SLOPE = 1.702
ROTARY_BASE = 10000.0
NEGATIVE = -1e30


def sent_together(arrays, axis, dim, along):
    columns = [a.reshape(*a.shape[:along], -1) for a in arrays]
    both = jnp.concatenate(columns, axis=along)
    out, at, done = (lax.all_gather(both, axis, axis=dim, tiled=True), 0, [])
    for a, column in zip(arrays, columns):
        share = out[..., at : at + column.shape[along]]
        done.append(share.reshape(*share.shape[:along], *a.shape[along:]))
        at += column.shape[along]
    return tuple(done)


def padded_to(lines, length):
    spare = -len(lines) % length
    return jnp.pad(lines, [(0, spare)] + [(0, 0)] * (lines.ndim - 1))


def sum_in_order(pieces, axes, turns):
    inside = pieces.shape[1:]
    pieces = pieces.reshape(*(lax.axis_size(a) for a in axes), *inside)
    pieces = jnp.moveaxis(pieces, turns, range(len(axes))).reshape(-1, *inside)
    for k in turns:
        pieces = lax.psum_scatter(pieces, axes[k], scatter_dimension=0, tiled=True)
    return pieces[0]


def gather_in_order(shard, axes, turns):
    pieces = shard[None]
    for k in turns:
        pieces = lax.all_gather(pieces, axes[k], axis=0, tiled=True)
    block = [lax.axis_size(axes[k]) for k in reversed(turns)]
    pieces = pieces.reshape(*block, *shard.shape)
    turned = sorted(range(len(turns)), key=lambda place: turns[len(turns) - 1 - place])
    return pieces.transpose(*turned, *range(len(turns), pieces.ndim)).reshape(-1, *shard.shape)


def sum_by_parts(shard, axes, turns):
    length, lines = (lax.axis_size(axes), shard.reshape(-1, *shard.shape[1:][-1:]))
    pieces = padded_to(lines, length).reshape(length, -1, *lines.shape[1:])
    own = sum_in_order(pieces, axes, turns)
    whole = gather_in_order(own, axes, turns[::-1]).reshape(-1, *lines.shape[1:])
    return whole[: len(lines)].reshape(shard.shape)


def sum_by_parts_2(shard, axis):
    lines = shard.reshape(-1, *shard.shape[1:][-1:])
    padded = padded_to(lines, lax.axis_size(axis))
    own = lax.psum_scatter(padded, axis, scatter_dimension=0, tiled=True)
    whole = lax.all_gather(own, axis, axis=0, tiled=True)
    return whole[: len(lines)].reshape(shard.shape)


def norm_rows(values, gains):
    widened = values.astype(jnp.float32)
    normed = widened * lax.rsqrt(jnp.mean(widened * widened, axis=-1, keepdims=True) + EPSILON)
    return (normed * gains).astype(jnp.bfloat16)


def rotary(values, position):
    half_dim = values.shape[-1] // 2
    frequency = ROTARY_BASE ** (-2.0 * jnp.arange(half_dim, dtype=jnp.float32) / values.shape[-1])
    angles = position.astype(jnp.float32)[:, None, None] * frequency[None, None, :]
    cosine = jnp.cos(angles)
    sine_part = jnp.sin(angles)
    lower = values[..., :half_dim]
    upper = values[..., half_dim:]
    return jnp.concatenate(
        [lower * cosine - upper * sine_part, upper * cosine + lower * sine_part], axis=-1
    )


def mixer_part(
    query_latent,
    shared_latent,
    rotary_key,
    query_gain,
    shared_gain,
    query_plain_weight,
    query_turn_weight,
    key_weight,
    value_weight,
    mixer_out_weight,
):
    row_count = query_latent.shape[0]
    head_count = query_plain_weight.shape[1] // NOPE
    position = lax.axis_index("ep") * row_count + jnp.arange(row_count, dtype=jnp.int32)
    query_normed = norm_rows(query_latent, query_gain)
    shared_normed = norm_rows(shared_latent, shared_gain)
    query_plain = jnp.dot(query_normed, query_plain_weight, preferred_element_type=jnp.float32)
    query_plain = query_plain.astype(jnp.bfloat16).reshape(row_count, head_count, NOPE)
    query_raw = jnp.dot(query_normed, query_turn_weight, preferred_element_type=jnp.float32)
    query_turned = rotary(query_raw.reshape(row_count, head_count, ROPE), position).astype(
        jnp.bfloat16
    )
    key_turned = rotary(rotary_key.astype(jnp.float32).reshape(row_count, 1, ROPE), position)
    key_turned = key_turned.astype(jnp.bfloat16).reshape(row_count, ROPE)
    scaling = (NOPE + ROPE) ** (-0.5)
    own_keys = jnp.dot(shared_normed, key_weight, preferred_element_type=jnp.float32)
    own_keys = own_keys.astype(jnp.bfloat16).reshape(row_count, head_count, NOPE)
    own_values = jnp.dot(shared_normed, value_weight, preferred_element_type=jnp.float32)
    own_values = own_values.astype(jnp.bfloat16).reshape(row_count, head_count, VDIM)
    portion = sent_together((own_keys, own_values, key_turned), "ep", 0, 1)
    key_plain = portion[0]
    key_total = key_plain.shape[0]
    peak_old = jnp.full((head_count, row_count), NEGATIVE, jnp.float32)
    scores = jnp.einsum("qhd,khd->hqk", query_plain, key_plain, preferred_element_type=jnp.float32)
    scores = scores + jnp.einsum(
        "qhr,kr->hqk", query_turned, portion[2], preferred_element_type=jnp.float32
    )
    scores = scores * scaling
    key_position = jnp.arange(key_total, dtype=jnp.int32)
    visible = (key_position[None, :] <= position[:, None])[None]
    scores = jnp.where(visible, scores, NEGATIVE)
    peak_new = jnp.maximum(peak_old, jnp.max(scores, axis=-1))
    weight = jnp.where(visible, jnp.exp(scores - peak_new[..., None]), 0.0)
    totals_new = jnp.sum(weight, axis=-1)
    accum_new = jnp.einsum(
        "hqk,khd->hqd", weight.astype(jnp.bfloat16), portion[1], preferred_element_type=jnp.float32
    )
    folded = (peak_new, totals_new, accum_new)
    peak_final, totals_final, accum_final = folded
    heads_out = accum_final / totals_final[..., None]
    heads_out = (
        jnp.transpose(heads_out, (1, 0, 2))
        .reshape(row_count, head_count * VDIM)
        .astype(jnp.bfloat16)
    )
    partial_value = jnp.dot(heads_out, mixer_out_weight, preferred_element_type=jnp.float32)
    return (
        sum_by_parts(partial_value.astype(jnp.bfloat16), TP, (0, 1))
        .astype(jnp.float32)
        .astype(jnp.bfloat16)
    )


def expert_part(
    expert_input, expert_gain, routing, routing_weight, gate_weight, up_weight, down_weight
):
    token_count = expert_input.shape[0]
    top_count = routing.shape[1]
    width = expert_input.shape[1]
    experts = lax.axis_size("ep")
    capacity = 4 * token_count * top_count // (3 * experts)
    normed = norm_rows(expert_input, expert_gain)
    flattened = routing.reshape(token_count * top_count)
    matches = (flattened[:, None] == jnp.arange(experts, dtype=jnp.int32)[None, :]).astype(
        jnp.int32
    )
    ranking = jnp.cumsum(matches, axis=0) - 1
    slot_index = jnp.sum(ranking * matches, axis=1)
    target = (flattened * capacity + slot_index).reshape(token_count, top_count)
    slot_ids = jnp.arange(experts * capacity, dtype=jnp.int32)
    select = target[None, :, :] == slot_ids[:, None, None]
    gather_table = jnp.any(select, axis=2).astype(jnp.bfloat16)
    outgoing = jnp.dot(gather_table, normed, preferred_element_type=jnp.float32).astype(
        jnp.bfloat16
    )
    outgoing = outgoing.reshape(experts, capacity, width)
    arrived = lax.all_to_all(outgoing, "ep", split_axis=0, concat_axis=0, tiled=True).reshape(
        experts * capacity, width
    )
    gate_local = gate_weight[0]
    up_local = up_weight[0]
    down_local = down_weight[0]
    gate_pre = jnp.minimum(
        jnp.dot(arrived, gate_local, preferred_element_type=jnp.float32), CLAMP_LIMIT
    )
    up_pre = jnp.clip(
        jnp.dot(arrived, up_local, preferred_element_type=jnp.float32), -CLAMP_LIMIT, CLAMP_LIMIT
    )
    hidden = ((up_pre + 1.0) * (gate_pre * jax.nn.sigmoid(SLOPE * gate_pre))).astype(jnp.bfloat16)
    partial_value = jnp.dot(hidden, down_local, preferred_element_type=jnp.float32)
    summed = sum_by_parts_2(partial_value.astype(jnp.bfloat16), TP).astype(jnp.float32)
    summed = summed.astype(jnp.bfloat16).reshape(experts, capacity, width)
    returned_rows = lax.all_to_all(summed, "ep", split_axis=0, concat_axis=0, tiled=True).reshape(
        experts * capacity, width
    )
    mixing = jnp.transpose(jnp.sum(jnp.where(select, routing_weight[None, :, :], 0.0), axis=2))
    result = jnp.dot(mixing, returned_rows.astype(jnp.float32))
    return result.astype(jnp.bfloat16)


def per_device(
    query_latent,
    shared_latent,
    rotary_key,
    query_gain,
    shared_gain,
    query_plain_weight,
    query_turn_weight,
    key_weight,
    value_weight,
    mixer_out_weight,
    expert_input,
    expert_gain,
    routing,
    routing_weight,
    gate_weight,
    up_weight,
    down_weight,
):
    mixer_output = mixer_part(
        query_latent,
        shared_latent,
        rotary_key,
        query_gain,
        shared_gain,
        query_plain_weight,
        query_turn_weight,
        key_weight,
        value_weight,
        mixer_out_weight,
    )
    expert_output = expert_part(
        expert_input, expert_gain, routing, routing_weight, gate_weight, up_weight, down_weight
    )
    return (mixer_output, expert_output)


def solution(mesh):
    finer = Mesh(mesh.devices.reshape(mesh.shape["ep"], 8, 2), ("ep", "tp_0", "tp_1"))
    placed = (
        P("ep", None),
        P("ep", None),
        P("ep", None),
        P(),
        P(),
        P(None, TP),
        P(None, TP),
        P(None, TP),
        P(None, TP),
        P(TP, None),
        P("ep", None),
        P(),
        P("ep", None),
        P("ep", None),
        P("ep", None, TP),
        P("ep", None, TP),
        P("ep", TP, None),
    )
    return jax.shard_map(
        per_device,
        mesh=finer,
        in_specs=placed,
        out_specs=(P("ep", None), P("ep", None)),
        check_vma=False,
    )
```

profile of v0, /device:TPU:1, one launch (start us, length us, event | category | flops | bytes accessed | tf_op | source)
XLA Modules:
  0.0 360.6 jit_solution(4953756799054424215)
XLA Ops:
  7.3 1.2 fusion.33
  9.3 1.1 fusion.36
  10.4 1.3 convolution_convert_fusion.4
  11.7 1.3 convolution_convert_fusion.5
  13.0 1.3 convolution_bitcast_fusion.2
  15.3 0.8 copy.44
  16.3 1.2 reduce-window.6
  19.1 2.0 convolution_convert_fusion.1
  21.1 2.5 reshape.278
  23.7 96.9 %all_to_all.10 = bf16[32,21,2048]{2,1,0:T(8,128)(2,1)} all-to-all(bf16[32,21,2048]{2,1,0:T(8,128)(2,1)} %reshape.278), channel_id=1, replica_groups=mesh['ep'=32,'tp_0'=8,'tp_1'=2] {'ep'}, dimensions={0} | all-to-all | bytes 5505024 | tf_op jit(solution)/shard_map/all_to_all | solution.py:177
  120.6 3.1 reshape.279
  123.7 2.6 convolution_minimum_fusion
  126.3 5.6 %convolution_convert_fusion = bf16[672,2048]{1,0:T(8,128)(2,1)} fusion(bf16[672,2048]{1,0:T(8,128)(2,1)S(1)} %reshape.279, bf16[1,128,2048]{2,1,0:T(8,128)(2,1)S(1)} %copy-done, bf16[1,2048,128]{2,1,0:T(8,128)(2,1)} %param.32, f32[672,128]{1,0:T(8,128)} %convolution_minimum_fusion), kind=kOutput, calls=%fused_computation.11 | convolution fusion | flops 706793472 | bytes 6897664 | tf_op jit(solution)/shard_map/dot_general | solution.py:190
  132.0 34.3 %fusion = bf16[48,2048]{1,0:T(8,128)(2,1)S(1)} fusion(bf16[672,2048]{1,0:T(8,128)(2,1)} %convolution_convert_fusion), kind=kCustom, calls=%all-reduce-scatter | all-reduce-scatter fusion | flops 1572865 | bytes 2951168
  166.3 2.9 collective-permute-start
  169.3 1.3 collective-permute-start.1
  170.6 1.3 dynamic-slice.4
  172.5 2.3 collective-permute-done.1
  176.4 6.3 %convolution_bitcast_fusion.1 = f32[1,256,8192]{2,1,0:T(8,128)} fusion(bf16[8192,320]{0,1:T(8,128)(2,1)} %all-gather.5.cloned.1.call-done, bf16[768,128]{1,0:T(8,128)(2,1)S(1)} %copy-done.3, bf16[256,768]{1,0:T(8,128)(2,1)S(1)} %copy-done.2, f32[768]{0:T(1024)S(1)} %copy-done.5, f32[256]{0:T(256)S(1)} %add_rsqrt_fusion.1), kind=kOutput, calls=%fused_computation.1 | convolution fusion | flops 588021760 | bytes 11079680 | tf_op jit(solution)/shard_map/qhd,khd->hqk/dot_general | solution.py:124
  182.7 6.9 %fusion.96 = (f32[256]{0:T(256)S(1)}, f32[1,256,8192]{2,1,0:T(8,128)}) fusion(f32[1,256,8192]{2,1,0:T(8,128)} %convolution_bitcast_fusion.1, bf16[256,32]{0,1:T(8,128)(2,1)S(1)} %get-tuple-element.3, bf16[256,32]{0,1:T(8,128)(2,1)S(1)} %get-tuple-element.2, bf16[8192,320]{0,1:T(8,128)(2,1)} %all-gather.5.cloned.1.call-done, s32[256]{0:T(256)S(1)} %iota_add_fusion), kind=kOutput, calls=%fused_computation.113 | convolution fusion | flops 278986496 | bytes 17860608 | tf_op jit(solution)/shard_map/qhr,kr->hqk/dot_general | solution.py:125
  189.6 31.8 %all-gather.9.cloned.1.call-done = bf16[16,42,2048]{2,1,0:T(8,128)(2,1)} async-done(((bf16[1,42,2048]{2,1,0:T(8,128)(2,1)}), bf16[16,42,2048]{2,1,0:T(8,128)(2,1)}) %all-gather.9.cloned.1.call-update) | async-done | bytes 2752528 | tf_op jit(solution)/shard_map/all_gather | solution.py:67
  221.4 5.3 %reshape.280 = bf16[32,21,2048]{2,1,0:T(8,128)(2,1)} reshape(bf16[16,42,2048]{2,1,0:T(8,128)(2,1)} %all-gather.9.cloned.1.call-done) | data formatting | bytes 5505024 | tf_op jit(solution)/shard_map/reshape | solution.py:192
  226.8 10.0 %all-to-all-start.1 = ((bf16[32,21,2048]{2,1,0:T(8,128)(2,1)}), bf16[32,21,2048]{2,1,0:T(8,128)(2,1)}, u32[]{:S(2)}, u32[]{:S(2)}) async-start(bf16[32,21,2048]{2,1,0:T(8,128)(2,1)} %reshape.280), calls=%async_computation.3 | async-start | bytes 6291456 | tf_op jit(solution)/shard_map/all_to_all | solution.py:193
  237.1 4.7 %fusion.4 = f32[256]{0:T(256)S(1)} fusion(f32[1,256,8192]{2,1,0:T(8,128)} %get-tuple-element.9, f32[256]{0:T(256)S(1)} %broadcast_maximum_fusion, s32[256]{0:T(256)S(1)} %iota_add_fusion), kind=kLoop, calls=%fused_computation.7 | loop fusion | flops 8388352 | bytes 8391680 | tf_op jit(solution)/shard_map/reduce_sum | solution.py:134
  241.7 7.5 %convolution_convert_fusion.2 = bf16[256,2048]{1,0:T(8,128)(2,1)} fusion(bf16[128,2048]{1,0:T(8,128)(2,1)S(1)} %copy-done.7, bf16[8192,320]{0,1:T(8,128)(2,1)} %all-gather.5.cloned.1.call-done, f32[1,256,8192]{2,1,0:T(8,128)} %get-tuple-element.9, f32[256]{0:T(256)S(1)} %broadcast_maximum_fusion, s32[256]{0:T(256)S(1)} %iota_add_fusion, f32[256]{0:T(256)S(1)} %fusion.4), kind=kOutput, calls=%fused_computation.13 | convolution fusion | flops 680067072 | bytes 12061696 | tf_op jit(solution)/shard_map/dot_general | solution.py:146
  249.3 35.9 %reduce-scatter.5.cloned.1.call-done = bf16[2,16,2048]{2,1,0:T(8,128)(2,1)} async-done(((bf16[16,16,2048]{2,1,0:T(8,128)(2,1)}), bf16[2,16,2048]{2,1,0:T(8,128)(2,1)}) %reduce-scatter.5.cloned.1.call-update) | async-done | bytes 131088 | tf_op jit(solution)/shard_map/reduce_scatter | solution.py:41
  285.2 22.7 %reduce-scatter.7.cloned.1.call-done = bf16[1,16,2048]{2,1,0:T(8,128)(2,1)} async-done(((bf16[2,16,2048]{2,1,0:T(8,128)(2,1)}), bf16[1,16,2048]{2,1,0:T(8,128)(2,1)}) %reduce-scatter.7.cloned.1.call-update) | async-done | bytes 65552 | tf_op jit(solution)/shard_map/reduce_scatter | solution.py:41
  307.9 3.3 all_gather.13
  311.4 35.9 %all-gather.7.cloned.1.call-done = bf16[16,16,2048]{2,1,0:T(8,128)(2,1)} async-done(((bf16[2,16,2048]{2,1,0:T(8,128)(2,1)}), bf16[16,16,2048]{2,1,0:T(8,128)(2,1)}) %all-gather.7.cloned.1.call-update) | async-done | bytes 1048592 | tf_op jit(solution)/shard_map/all_gather | solution.py:48
  347.4 3.0 reshape.281
  350.4 1.4 fusion.97
  351.8 2.3 copy.52
  (55 shorter events, 5.8 us)
Async XLA Ops:
  7.2 119.2 %copy-start = (bf16[1,128,2048]{2,1,0:T(8,128)(2,1)S(1)}, bf16[1,128,2048]{2,1,0:T(8,128)(2,1)}, u32[]{:S(2)}) copy-start(bf16[1,128,2048]{2,1,0:T(8,128)(2,1)} %param.33) | copy-start | bytes 1572868
  7.2 11.6 %copy-start.1 = (bf16[128,2048]{1,0:T(8,128)(2,1)S(1)}, bf16[128,2048]{1,0:T(8,128)(2,1)}, u32[]{:S(2)}) copy-start(bf16[128,2048]{1,0:T(8,128)(2,1)} %param.27) | copy-start | bytes 1572868
  7.2 11.9 %copy-start.4 = (f32[2048]{0:T(1024)S(1)}, f32[2048]{0:T(1024)}, u32[]{:S(2)}) copy-start(f32[2048]{0:T(1024)} %param.28) | copy-start | bytes 24580
  7.2 169.1 %all-gather.5.cloned.1.call-start = ((), (), s32[]{:S(2)}) async-start(), calls=%async_computation.4 | async-start | bytes 5406720 | tf_op jit(solution)/shard_map/all_gather | solution.py:23
  15.3 206.2 %all-gather.9.cloned.1.call-start = ((), (), s32[]{:S(2)}) async-start(), calls=%async_computation.8 | async-start | bytes 3342336 | tf_op jit(solution)/shard_map/all_gather | solution.py:67
  132.0 44.4 %copy-start.2 = (bf16[256,768]{1,0:T(8,128)(2,1)S(1)}, bf16[256,768]{1,0:T(8,128)(2,1)}, u32[]{:S(2)}) copy-start(bf16[256,768]{1,0:T(8,128)(2,1)} %param.17) | copy-start | bytes 1179652
  132.0 44.4 %copy-start.3 = (bf16[768,128]{1,0:T(8,128)(2,1)S(1)}, bf16[768,128]{1,0:T(8,128)(2,1)}, u32[]{:S(2)}) copy-start(bf16[768,128]{1,0:T(8,128)(2,1)} %param.22) | copy-start | bytes 589828
  132.0 44.4 %copy-start.5 = (f32[768]{0:T(1024)S(1)}, f32[768]{0:T(1024)}, u32[]{:S(2)}) copy-start(f32[768]{0:T(1024)} %param.20) | copy-start | bytes 9220
  166.3 8.5 %collective-permute-start = (bf16[48,2048]{1,0:T(8,128)(2,1)S(1)}, bf16[48,2048]{1,0:T(8,128)(2,1)S(1)}, u32[]{:S(2)}, u32[]{:S(2)}) collective-permute-start(bf16[48,2048]{1,0:T(8,128)(2,1)S(1)} %fusion), channel_id=1, source_target_pairs={{0,1},{1,2},{2,3},{3,4},{4,5},{5,6},{6,7},{7,8},{8,9},{9,10},{10,1... | collective-permute-start | bytes 589832
  169.3 5.5 %collective-permute-start.1 = (bf16[42,2048]{1,0:T(8,128)(2,1)S(1)}, bf16[42,2048]{1,0:T(8,128)(2,1)S(1)}, u32[]{:S(2)}, u32[]{:S(2)}) collective-permute-start(bf16[42,2048]{1,0:T(8,128)(2,1)S(1)} %slice.44), channel_id=1, source_target_pairs={{0,2},{1,3},{2,4},{3,5},{4,6},{5,7},{6,8},{7,9},{8,10},{9,11},{10,... | collective-permute-start | bytes 516104
  226.8 120.6 %all-to-all-start.1 = ((bf16[32,21,2048]{2,1,0:T(8,128)(2,1)}), bf16[32,21,2048]{2,1,0:T(8,128)(2,1)}, u32[]{:S(2)}, u32[]{:S(2)}) async-start(bf16[32,21,2048]{2,1,0:T(8,128)(2,1)} %reshape.280), calls=%async_computation.3 | async-start | bytes 6291456 | tf_op jit(solution)/shard_map/all_to_all | solution.py:193
  236.8 48.3 %reduce-scatter.5.cloned.1.call-start = ((), (), s32[]{:S(2)}) async-start(), calls=%async_computation.5 | async-start | bytes 1179648 | tf_op jit(solution)/shard_map/reduce_scatter | solution.py:41
  237.0 4.7 %copy-start.7 = (bf16[128,2048]{1,0:T(8,128)(2,1)S(1)}, bf16[128,2048]{1,0:T(8,128)(2,1)}, u32[]{:S(2)}) copy-start(bf16[128,2048]{1,0:T(8,128)(2,1)} %param.26) | copy-start | bytes 1572868
  241.7 69.5 %copy-start.6 = (f32[128,4]{0,1:T(4,128)S(1)}, f32[128,4]{0,1:T(4,128)}, u32[]{:S(2)}) copy-start(f32[128,4]{0,1:T(4,128)} %param.30) | copy-start | bytes 6148
  249.2 58.7 %reduce-scatter.7.cloned.1.call-start = ((), (), s32[]{:S(2)}) async-start(), calls=%async_computation.6 | async-start | bytes 196608 | tf_op jit(solution)/shard_map/reduce_scatter | solution.py:41
  285.2 62.2 %all-gather.7.cloned.1.call-start = ((), (), s32[]{:S(2)}) async-start(), calls=%async_computation.7 | async-start | bytes 1179648 | tf_op jit(solution)/shard_map/all_gather | solution.py:48
Sparse Core Ops, SparseCore 0:
  15.4 129.1 all-gather.4
  176.4 44.9 all-gather.8
  249.3 35.7 reduce-scatter.4
  287.8 20.0 reduce-scatter.6
  311.4 35.9 all-gather.6
where the time goes:
time: 366 us; the launch traced here: 361 us
  blocking collectives  135 us (37%)
  waiting for transfers between devices  129 us (35%)
  matrix products  36.3 us (10%)
  local copies, waits for them, and re-layouts  20.5 us (6%)
  between operations  14.7 us (4%)
  starting transfers between devices  14.6 us (4%)
  other arithmetic  11.2 us (3%)
    all_to_all x1, blocking collectives, expert_part(): lax.all_to_all(outgoing, 'ep', split_axis=0, concat_axis=0, tiled=True)  96.9 us
    reduce_scatter x2, waiting for transfers between devices, sum_in_order(): pieces = lax.psum_scatter(pieces, axes[k], scatter_dimension=0, tiled=True)  58.6 us
    all_gather x1, waiting for transfers between devices, gather_in_order(): pieces = lax.all_gather(pieces, axes[k], axis=0, tiled=True)  35.9 us
    unnamed x1, blocking collectives  34.3 us
    all_gather x1, waiting for transfers between devices, sum_by_parts_2(): whole = lax.all_gather(own, axis, axis=0, tiled=True)  31.8 us
    all_to_all x1, starting transfers between devices, expert_part(): lax.all_to_all(summed, 'ep', split_axis=0, concat_axis=0, tiled=True)  10 us
    dot_general x1, matrix products, mixer_part(): jnp.dot(heads_out, mixer_out_weight, preferred_element_type=jnp.float32)  7.46 us
  transfers between devices with their start and end apart: 8, of which 5 were waited for; matrix products, arithmetic and copies ran while one was open for 23% of the time, Pallas kernels for 0%

commit v1 on v0

v1 whole, which is shorter than its diff:
```python
import functools
import math

import jax
import jax.numpy as jnp
from jax import lax
from jax.experimental import pallas as pl
from jax.experimental.pallas import tpu as pltpu
from jax.sharding import Mesh
from jax.sharding import PartitionSpec as P

MESH = pl.DeviceIdType.MESH
F32 = jnp.float32
BF16 = jnp.bfloat16
NOPE = 128
ROPE = 64
LANES = 128
EPSILON = 1e-06
CLAMP_LIMIT = 7.0
SLOPE = 1.702
ROTARY_BASE = 10000.0
NEGATIVE = -1e30
EP = ("z", "x")
TP = ("y", "c")
NX = 4


def dot(a, b, on_a=1, on_b=0):
    return lax.dot_general(a, b, (((on_a,), (on_b,)), ((), ())), preferred_element_type=F32)


def iota(shape, dim):
    return lax.broadcasted_iota(jnp.int32, shape, dim)


def normed(ref, gain_ref):
    wide = ref[...].astype(F32)
    wide = wide * lax.rsqrt(jnp.mean(wide * wide, axis=-1, keepdims=True) + EPSILON)
    return (wide * gain_ref[...]).astype(BF16)


def turned(u, cosine, sine):
    half = u.shape[0] // 2
    lower, upper = u[:half], u[half:]
    return jnp.concatenate([lower * cosine - upper * sine, upper * cosine + lower * sine], axis=0)


class Sender:
    def __init__(self):
        self.owed = []

    def copy(self, src, dst, send_sem, recv_sem, device):
        return pltpu.make_async_remote_copy(
            src_ref=src, dst_ref=dst, send_sem=send_sem, recv_sem=recv_sem,
            device_id=device, device_id_type=MESH,
        )

    def start(self, *what):
        made = self.copy(*what)
        made.start()
        self.owed.append(made.wait_send)

    def finish(self):
        for wait in self.owed:
            wait()


def ring_gather(send, axis, size, buf, slot, send_sem, recv_sem, pair=None):
    me = lax.axis_index(axis)
    ways = ({axis: lax.rem(me + 1, size)}, {axis: lax.rem(me + size - 1, size)})
    steps = size // 2
    rows = buf.shape[1] // 2

    def part(offset, half):
        return buf.at[slot(lax.rem(me + offset + size, size)), pl.ds(half * rows, rows)]

    def in_use(step, way, half):
        return step < steps or way == half

    def hop(step, way, half):
        ref = part((1 - step) if way == 0 else (step - 1), half)
        at = (way, step - 1, half)
        return (ref, ref, send_sem.at[at], recv_sem.at[at], ways[way])

    def hand(ref, at):
        if pair is not None:
            device, pair_send, pair_recv = pair
            send.start(ref, ref, pair_send.at[at], pair_recv.at[at], device)

    for half in range(2):
        for way in range(2):
            if in_use(1, way, half):
                send.start(*hop(1, way, half))
    if pair is not None:
        for half in range(2):
            hand(part(0, half), (0, steps, half))
    yield
    for step in range(1, steps + 1):
        for half in range(2):
            for way in range(2):
                if in_use(step, way, half):
                    at = (way, step - 1, half)
                    ref = part(-step if way == 0 else step, half)
                    send.copy(ref, ref, send_sem.at[at], recv_sem.at[at], ways[way]).wait_recv()
                    if step < steps and in_use(step + 1, way, half):
                        send.start(*hop(step + 1, way, half))
                    hand(ref, at)
        yield


def pair_arrived(send, size, axis, buf, slot, step, pair):
    device, pair_send, pair_recv = pair
    me = lax.axis_index(axis)
    steps = size // 2
    rows = buf.shape[1] // 2
    if step == 0:
        todo = [((0, steps, half), 0, half) for half in range(2)]
    else:
        todo = [
            ((way, step - 1, half), -step if way == 0 else step, half)
            for half in range(2) for way in range(2) if step < steps or way == half
        ]
    for at, offset, half in todo:
        ref = buf.at[slot(lax.rem(me + offset + size, size)), pl.ds(half * rows, rows)]
        send.copy(ref, ref, pair_send.at[at], pair_recv.at[at], device).wait_recv()


def product_scatter(send, size, product, part, given, ring, sems, pair_device, result):
    pair_send, pair_recv, send_sem, recv_sem = sems
    me, core = lax.axis_index("y"), lax.axis_index("c")
    ways = ({"y": lax.rem(me + 1, size)}, {"y": lax.rem(me + size - 1, size)})
    steps = size // 2
    rows = part.shape[2] // 2
    order = [steps]
    for k in range(steps - 1, 0, -1):
        order += [k, -k]
    order += [0]
    place = {offset % size: i for i, offset in enumerate(order)}
    seen = set()

    def at_piece(offset):
        return lax.rem(me + offset + size, size)

    def given_copy(offset):
        p, i = at_piece(offset), place[offset % size]
        return (part.at[1 - core, p], given.at[p], pair_send.at[i], pair_recv.at[i], pair_device)

    for offset in order:
        p = at_piece(offset)
        both = product(p).astype(BF16)
        part[0, p] = both[:, :LANES]
        part[1, p] = both[:, LANES:]
        send.start(*given_copy(offset))

    def in_use(step, way, half):
        return step >= 2 or way == half

    def arrival(step, way, half):
        at = (way, step - 1, half)
        ref = ring.at[way, step - 1, pl.ds(half * rows, rows)]
        send.copy(ref, ref, send_sem.at[at], recv_sem.at[at], ways[way]).wait_recv()
        return ring[way, step - 1, pl.ds(half * rows, rows)].astype(F32)

    def own(offset, half):
        if offset % size not in seen:
            seen.add(offset % size)
            send.copy(*given_copy(offset)).wait_recv()
        p, where = at_piece(offset), pl.ds(half * rows, rows)
        return part[core, p, where].astype(F32) + given[p, where].astype(F32)

    yield
    for step in range(1, steps + 1):
        for half in range(2):
            for way in range(2):
                if in_use(step, way, half):
                    offset = (steps - step + 1) * (1 if way == 0 else -1)
                    value = own(offset, half)
                    if step > 1 and in_use(step - 1, way, half):
                        value = value + arrival(step - 1, way, half)
                    p, where, at = at_piece(offset), pl.ds(half * rows, rows), (way, step - 1, half)
                    part[core, p, where] = value.astype(BF16)
                    send.start(
                        part.at[core, p, where], ring.at[way, step - 1, where],
                        send_sem.at[at], recv_sem.at[at], ways[way],
                    )
        yield
    for half in range(2):
        value = own(0, half)
        for way in range(2):
            if in_use(steps, way, half):
                value = value + arrival(steps, way, half)
        result[pl.ds(half * rows, rows)] = value.astype(BF16)


def exchange(send, nz, nx, src, dst, send_sem, recv_sem):
    count = nz * nx
    me = lax.axis_index("z") * nx + lax.axis_index("x")

    def out(d):
        to = lax.rem(me + d, count)
        return send.copy(
            src.at[to], dst.at[me], send_sem.at[d], recv_sem.at[d], {"z": to // nx, "x": lax.rem(to, nx)}
        )

    @pl.loop(1, count)
    def _(d):
        out(d).start()

    def wait():
        @pl.loop(1, count)
        def _(d):
            origin = lax.rem(me + count - d, count)
            send.copy(
                src.at[origin], dst.at[origin], send_sem.at[d], recv_sem.at[d],
                {"z": origin // nx, "x": lax.rem(origin, nx)},
            ).wait_recv()

    def sent():
        @pl.loop(1, count)
        def _(d):
            out(d).wait_send()

    send.owed.append(sent)
    dst[me] = src[me]
    return wait


def kernel(sizes, *refs):
    nz, nx, ny, cap, spaced = sizes
    (query_latent, shared_latent, rotary_key, cosine, sine, query_gain, shared_gain, plain_weight, turn_weight,
     key_weight, value_weight, mixer_weight, tokens, token_gain, routing, routing_weight, gate, up, down,
     mixer_out, expert_out, *scratch) = refs
    (out_rows, in_rows, pack, mix_high, mix_low, gath, gate_up, hidden, part_e, given_e, ring_e, back_out, back_in,
     result_e, queries, query_1, query_2, keys, peak, total, accum, share_out, stat_out, share_in, stat_in,
     heads, part_m, given_m, ring_m,
     s_a, r_a, s_g, r_g, sp_g, rp_g, sp_e, rp_e, s_e, r_e, s_b, r_b, s_f, r_f, sp_f, rp_f,
     s_q, r_q, s_k, r_k, s_o, r_o, s_t, r_t, sp_m, rp_m, s_m, r_m, s_h, r_h, sp_h, rp_h) = scratch
    z, x, y, core = (lax.axis_index(a) for a in ("z", "x", "y", "c"))
    count = nz * nx
    me = z * nx + x
    turn = 2 * y + core
    rows = query_latent.shape[0]
    other = {"c": 1 - core}
    send = Sender()

    barrier = pltpu.get_barrier_semaphore()

    @pl.loop(1, count)
    def _(d):
        to = lax.rem(me + d, count)
        pl.semaphore_signal(
            barrier, inc=1, device_id={"z": to // nx, "x": lax.rem(to, nx)}, device_id_type=MESH
        )

    for device in ({"y": lax.rem(y + 1, ny)}, {"y": lax.rem(y + ny - 1, ny)}, other):
        pl.semaphore_signal(barrier, inc=1, device_id=device, device_id_type=MESH)

    def expert_chain():
        width = pl.ds(pl.multiple_of(turn * LANES, LANES), LANES)
        wide = tokens[...].astype(F32)
        factor = lax.rsqrt(jnp.mean(wide * wide, axis=-1, keepdims=True) + EPSILON)
        own = (tokens[:, width].astype(F32) * factor * token_gain[:, width]).astype(BF16)
        count_of = own.shape[0]
        named = iota((count, count_of), 0)
        member = jnp.zeros((count, count_of), F32)
        weight = jnp.zeros((count, count_of), F32)
        for k in range(routing.shape[0]):
            hit = routing[k : k + 1, :] == named
            member = member + jnp.where(hit, 1.0, 0.0)
            weight = weight + jnp.where(hit, routing_weight[k : k + 1, :], 0.0)
        member = member.astype(BF16)
        earlier = jnp.where(
            iota((count_of, count_of), 0) < iota((count_of, count_of), 1), 1.0, 0.0
        ).astype(BF16)
        rank = dot(member, earlier).astype(BF16)
        slots = count * spaced
        shift = spaced.bit_length() - 1
        spread = jnp.where(
            lax.shift_right_logical(iota((slots, count), 0), shift) == iota((slots, count), 1), 1.0, 0.0
        ).astype(BF16)
        place = (iota((slots, count_of), 0) & (spaced - 1)).astype(F32)
        chosen = (dot(spread, member) > 0.5) & (dot(spread, rank) == place)
        high = weight.astype(BF16)
        low = (weight - high.astype(F32)).astype(BF16)
        mix_high[...] = jnp.where(chosen, dot(spread, high), 0.0).astype(BF16)
        mix_low[...] = jnp.where(chosen, dot(spread, low), 0.0).astype(BF16)
        out_rows[...] = dot(jnp.where(chosen, 1.0, 0.0).astype(BF16), own).astype(BF16).reshape(out_rows.shape)
        yield
        arrive = exchange(send, nz, nx, out_rows, in_rows, s_a, r_a)
        yield
        column = iota(pack.shape, 1)
        inner = column & (spaced - 1)
        goal = jnp.where(inner < cap, lax.shift_right_logical(column, shift) * cap + inner, -1)
        pack[...] = jnp.where(goal == iota(pack.shape, 0), 1.0, 0.0).astype(BF16)
        arrive()
        gath[turn] = dot(pack[...], in_rows[...].reshape(slots, LANES)).astype(BF16)
        slot = lambda p: 2 * p + core
        slot_other = lambda p: 2 * p + 1 - core
        pair = (other, sp_g, rp_g)
        ring = ring_gather(send, "y", ny, gath, slot, s_g, r_g, pair)
        steps = ny // 2
        next(ring)
        gate_up[...] = jnp.zeros_like(gate_up)

        def consume(piece):
            rows_of = pl.ds(pl.multiple_of(piece * LANES, LANES), LANES)
            both = jnp.concatenate([gate[rows_of, :], up[rows_of, :]], axis=1)
            gate_up[...] += dot(gath[piece], both)

        def consume_step(step, which):
            for offset in sorted({-step % ny, step % ny}):
                consume(which(lax.rem(y + offset, ny)))

        consume_step(0, slot)
        yield
        for step in range(1, steps + 1):
            next(ring)
            pair_arrived(send, ny, "y", gath, slot_other, step - 1, pair)
            consume_step(step - 1, slot_other)
            consume_step(step, slot)
            yield
        pair_arrived(send, ny, "y", gath, slot_other, steps, pair)
        consume_step(steps, slot_other)
        gate_pre = jnp.minimum(gate_up[:, :LANES], CLAMP_LIMIT)
        up_pre = jnp.clip(gate_up[:, LANES:], -CLAMP_LIMIT, CLAMP_LIMIT)
        hidden[...] = ((up_pre + 1.0) * (gate_pre * jax.nn.sigmoid(SLOPE * gate_pre))).astype(BF16)

        def product(p):
            return dot(hidden[...], down[:, pl.ds(pl.multiple_of(2 * LANES * p, 2 * LANES), 2 * LANES)])

        yield from product_scatter(
            send, ny, product, part_e, given_e, ring_e, (sp_e, rp_e, s_e, r_e), other, result_e
        )
        back_out[...] = dot(pack[...], result_e[...], 0, 0).astype(BF16).reshape(back_out.shape)
        arrive = exchange(send, nz, nx, back_out, back_in, s_b, r_b)
        yield
        arrive()
        back = back_in[...].reshape(slots, LANES)
        mixed = dot(mix_high[...], back, 0, 0) + dot(mix_low[...], back, 0, 0)
        expert_out[turn] = mixed.astype(BF16)
        pair = (other, sp_f, rp_f)
        yield from ring_gather(send, "y", ny, expert_out, slot, s_f, r_f, pair)
        for step in range(steps + 1):
            pair_arrived(send, ny, "y", expert_out, slot_other, step, pair)

    def mixer_chain():
        scale = (NOPE + ROPE) ** -0.5 * math.log2(math.e)
        latent = normed(query_latent, query_gain)
        queries[x, :rows] = dot(latent, plain_weight[...]).astype(BF16)
        raw = turned(dot(turn_weight[...], latent, 1, 1), cosine[...], sine[...])
        raw = jnp.concatenate([raw, jnp.zeros_like(raw)], axis=0)
        queries[x, rows:] = raw.T.astype(BF16)
        shared = normed(shared_latent, shared_gain)
        keys[z, :rows] = dot(shared, key_weight[...]).astype(BF16)
        keys[z, rows : 2 * rows] = dot(shared, value_weight[...]).astype(BF16)
        raw = turned(rotary_key[...].astype(F32), cosine[...], sine[...])
        raw = jnp.concatenate([raw[:, : rows // 2], raw[:, rows // 2 :]], axis=0)
        keys[z, 2 * rows :] = raw.T.astype(BF16)
        yield
        to_x = [lax.rem(x + d, nx) for d in range(nx)]
        from_x = [lax.rem(x + nx - d, nx) for d in range(nx)]
        for d in range(1, nx):
            send.start(queries.at[x], queries.at[x], s_q.at[d], r_q.at[d], {"x": to_x[d]})
        ring = ring_gather(send, "z", nz, keys, lambda p: p, s_k, r_k)
        next(ring)
        yield
        for d in range(1, nx):
            ref = queries.at[from_x[d]]
            send.copy(ref, ref, s_q.at[d], r_q.at[d], {"x": to_x[d]}).wait_recv()
        move = jnp.where(iota((LANES, LANES), 0) + ROPE == iota((LANES, LANES), 1), 1.0, 0.0).astype(BF16)
        for j in range(nx):
            span = pl.ds(j * rows, rows)
            plain, turned_part = queries[j, :rows], queries[j, rows:]
            query_1[span, :LANES] = plain
            query_1[span, LANES:] = turned_part
            query_2[span, :LANES] = plain
            query_2[span, LANES:] = dot(turned_part, move).astype(BF16)

        def attend(piece, own):
            half = rows // 2
            both = keys[piece, 2 * rows :]
            key_1 = jnp.concatenate([keys[piece, :half], both], axis=1)
            key_2 = jnp.concatenate([keys[piece, half:rows], both], axis=1)
            scores = jnp.concatenate(
                [dot(key_1, query_1[...], 1, 1), dot(key_2, query_2[...], 1, 1)], axis=0
            )
            if own:
                visible = iota(scores.shape, 0) + rows * x <= iota(scores.shape, 1)
                scores = jnp.where(visible, scores, NEGATIVE)
            highest = jnp.max(scores, axis=0, keepdims=True)
            if not own:
                highest = jnp.maximum(highest, peak[...])
            probs = jnp.exp2((scores - highest) * scale)
            summed = jnp.sum(probs, axis=0, keepdims=True)
            mixed = dot(keys[piece, rows : 2 * rows], probs.astype(BF16), 0, 0)
            if own:
                total[...] = summed
                accum[...] = mixed
            else:
                fade = jnp.exp2((peak[...] - highest) * scale)
                total[...] = total[...] * fade + summed
                accum[...] = accum[...] * fade + mixed
            peak[...] = highest

        attend(z, True)
        yield
        steps = nz // 2
        for step in range(1, steps + 1):
            next(ring)

            @pl.when(z >= step)
            def _():
                attend(lax.rem(z - step + nz, nz), False)

            if step < steps:
                @pl.when(z + step >= nz)
                def _():
                    attend(lax.rem(z + step, nz), False)

            yield
        share = (accum[...] / total[...]).astype(BF16)
        for j in range(nx):
            span = slice(j * rows, (j + 1) * rows)
            share_out[j] = share[:, span]
            stat = (8, rows)
            stat_out[j] = jnp.where(iota(stat, 0) == 0, peak[:, span], total[:, span])
        for d in range(1, nx):
            device = {"x": to_x[d]}
            send.start(share_out.at[to_x[d]], share_in.at[x], s_o.at[d], r_o.at[d], device)
            send.start(stat_out.at[to_x[d]], stat_in.at[x], s_t.at[d], r_t.at[d], device)
        share_in[x] = share_out[x]
        stat_in[x] = stat_out[x]
        yield
        for d in range(1, nx):
            device = {"x": to_x[d]}
            for ref, s, r in ((share_in, s_o, r_o), (stat_in, s_t, r_t)):
                ref = ref.at[from_x[d]]
                send.copy(ref, ref, s.at[d], r.at[d], device).wait_recv()
        peaks = [stat_in[j, 0:1, :] for j in range(nx)]
        highest = functools.reduce(jnp.maximum, peaks)
        factors = [stat_in[j, 1:2, :] * jnp.exp2((peaks[j] - highest) * scale) for j in range(nx)]
        merged = sum(share_in[j].astype(F32) * factors[j] for j in range(nx)) / sum(factors)
        heads[...] = merged.astype(BF16)

        def product(p):
            columns = pl.ds(pl.multiple_of(2 * LANES * p, 2 * LANES), 2 * LANES)
            return dot(heads[...], mixer_weight[:, columns], 0, 0)

        yield from product_scatter(
            send, ny, product, part_m, given_m, ring_m, (sp_m, rp_m, s_m, r_m), other, mixer_out.at[turn]
        )
        pair = (other, sp_h, rp_h)
        yield from ring_gather(send, "y", ny, mixer_out, lambda p: 2 * p + core, s_h, r_h, pair)
        for step in range(ny // 2 + 1):
            pair_arrived(send, ny, "y", mixer_out, lambda p: 2 * p + 1 - core, step, pair)

    chains = [expert_chain(), mixer_chain()]
    for chain in chains:
        next(chain)
    pl.semaphore_wait(barrier, count + 2)
    while chains:
        for chain in list(chains):
            try:
                next(chain)
            except StopIteration:
                chains.remove(chain)
    send.finish()


def per_device(sizes, query_latent, shared_latent, rotary_key, query_gain, shared_gain, plain_weight, turn_weight,
               key_weight, value_weight, mixer_weight, tokens, token_gain, routing, routing_weight, gate, up, down):
    nz, nx, ny, cap, spaced = sizes
    rows = query_latent.shape[0]
    position = (lax.axis_index(EP) * rows + jnp.arange(rows, dtype=jnp.int32)).astype(F32)
    half = ROPE // 2
    frequency = ROTARY_BASE ** (-2.0 * jnp.arange(half, dtype=F32) / ROPE)
    angles = position[None, :] * frequency[:, None]
    count, pieces = nz * nx, 2 * ny
    slots, packed = count * spaced, count * cap
    count_of = tokens.shape[0]
    vmem, dma = pltpu.VMEM, pltpu.SemaphoreType.DMA
    hops, handed = dma((2, ny // 2, 2)), dma((2, ny // 2 + 1, 2))
    scratch = [
        vmem((count, spaced, LANES), BF16), vmem((count, spaced, LANES), BF16), vmem((packed, slots), BF16),
        vmem((slots, count_of), BF16), vmem((slots, count_of), BF16), vmem((pieces, packed, LANES), BF16),
        vmem((packed, 2 * LANES), F32), vmem((packed, LANES), BF16), vmem((2, ny, packed, LANES), BF16),
        vmem((ny, packed, LANES), BF16), vmem((2, ny // 2, packed, LANES), BF16),
        vmem((count, spaced, LANES), BF16), vmem((count, spaced, LANES), BF16), vmem((packed, LANES), BF16),
        vmem((nx, 2 * rows, LANES), BF16), vmem((nx * rows, 2 * LANES), BF16), vmem((nx * rows, 2 * LANES), BF16),
        vmem((nz, 2 * rows + rows // 2, LANES), BF16), vmem((1, nx * rows), F32), vmem((1, nx * rows), F32),
        vmem((LANES, nx * rows), F32), vmem((nx, LANES, rows), BF16), vmem((nx, 8, rows), F32),
        vmem((nx, LANES, rows), BF16), vmem((nx, 8, rows), F32), vmem((LANES, rows), BF16),
        vmem((2, ny, rows, LANES), BF16), vmem((ny, rows, LANES), BF16), vmem((2, ny // 2, rows, LANES), BF16),
        dma((count,)), dma((count,)), hops, hops, handed, handed, dma((ny,)), dma((ny,)), hops, hops,
        dma((count,)), dma((count,)), hops, hops, handed, handed,
        dma((nx,)), dma((nx,)), dma((2, nz // 2, 2)), dma((2, nz // 2, 2)), dma((nx,)), dma((nx,)), dma((nx,)),
        dma((nx,)), dma((ny,)), dma((ny,)), hops, hops, hops, hops, handed, handed,
    ]
    spec = pl.BlockSpec(memory_space=pltpu.VMEM)
    operands = (
        query_latent, shared_latent, rotary_key.T, jnp.cos(angles), jnp.sin(angles), query_gain[None],
        shared_gain[None], plain_weight, turn_weight.T, key_weight, value_weight, mixer_weight, tokens,
        token_gain[None], routing.T, routing_weight.T, gate[0], up[0], down[0],
    )
    mixer_out, expert_out = pl.pallas_call(
        functools.partial(kernel, sizes),
        out_shape=(
            jax.ShapeDtypeStruct((pieces, rows, LANES), BF16),
            jax.ShapeDtypeStruct((pieces, count_of, LANES), BF16),
        ),
        in_specs=[spec] * len(operands),
        out_specs=(spec, spec),
        scratch_shapes=scratch,
        compiler_params=pltpu.CompilerParams(
            collective_id=0, has_side_effects=True, vmem_limit_bytes=56 * 1024 * 1024
        ),
        name="step",
    )(*operands)
    return tuple(a.transpose(1, 0, 2).reshape(a.shape[1], -1) for a in (mixer_out, expert_out))


def build(mesh, nx, cap, spaced):
    nz, ny = mesh.shape["ep"] // nx, mesh.shape["tp"] // 2
    finer = Mesh(mesh.devices.reshape(nz, nx, ny, 2), ("z", "x", "y", "c"))
    placed = (
        P(EP, None), P(EP, None), P(EP, None), P(), P(), P(None, TP), P(None, TP), P(None, TP), P(None, TP),
        P(TP, None), P(EP, None), P(), P(EP, None), P(EP, None), P(EP, None, TP), P(EP, None, TP), P(EP, TP, None),
    )
    return jax.shard_map(
        functools.partial(per_device, (nz, nx, ny, cap, spaced)),
        mesh=finer, in_specs=placed, out_specs=(P(EP, None), P(EP, None)), check_vma=False,
    )


def solution(mesh):
    return build(mesh, NX, 21, 32)
```

time: 366 us -> 112 us (0.31); the launches traced: 361 us -> 112 us
  blocking collectives: 135 us -> 0 us
  waiting for transfers between devices: 129 us -> 0 us
  Pallas kernels: 0 us -> 105 us
  matrix products: 36.3 us -> 0 us
  local copies, waits for them, and re-layouts: 20.5 us -> 5.44 us
  starting transfers between devices: 14.6 us -> 0 us
  between operations: 14.7 us -> 0.69 us
  other arithmetic: 11.2 us -> 0.84 us
    pallas_call x0 -> x1, Pallas kernels: none -> 105 us  [per_device(): pl.pallas_call(functools.partial(kernel, sizes), out_shape=(jax.ShapeDtyp...]
    all_to_all x1 -> x0, blocking collectives: 96.9 us -> none  [expert_part(): lax.all_to_all(outgoing, 'ep', split_axis=0, concat_axis=0, tiled=True)]
    all_gather x3 -> x0, waiting for transfers between devices: 67.8 us -> none  [the longest x1 35.9 us: gather_in_order(): pieces = lax.all_gather(pieces, axes[k], axis=0, tiled=True)]
    reduce_scatter x2 -> x0, waiting for transfers between devices: 58.6 us -> none  [sum_in_order(): pieces = lax.psum_scatter(pieces, axes[k], scatter_dimension=0, tiled=True)]
    dot_general x10 -> x0, matrix products: 36.3 us -> none  [the longest x1 7.46 us: mixer_part(): jnp.dot(heads_out, mixer_out_weight, preferred_element_type=jnp.float32)]
    unnamed x1 -> x0, blocking collectives: 34.3 us -> none
    reshape x4 -> x0, local copies, waits for them, and re-layouts: 14 us -> none  [the longest x1 5.35 us: expert_part(): summed = summed.astype(jnp.bfloat16).reshape(experts, capacity, width)]
    all_to_all x1 -> x0, starting transfers between devices: 10 us -> none  [expert_part(): lax.all_to_all(summed, 'ep', split_axis=0, concat_axis=0, tiled=True)]
  transfers between devices with their start and end apart: 8 -> 0, of which waited for: 5 -> 0; matrix products, arithmetic and copies ran while one was open for 23% -> 0% of each run, Pallas kernels for 0% -> 0%
where the time goes in v1:
time: 112 us
  Pallas kernels  105 us (94%)
  local copies, waits for them, and re-layouts  5.44 us (5%)
    pallas_call x1, Pallas kernels, per_device(): pl.pallas_call(functools.partial(kernel, sizes), out_shape=(jax.ShapeDtyp...  105 us
    unnamed x6, local copies, waits for them, and re-layouts  3.09 us

profile of v1, /device:TPU:1, one launch (start us, length us, event | category | flops | bytes accessed | tf_op | source)
XLA Modules:
  0.0 112.3 jit_solution(8997966369357340029)
XLA Ops:
  0.6 0.0 copy-start.1
  0.7 0.7 copy-done.1
  1.3 0.6 broadcast_in_dim.11.refs_5_
  1.9 0.8 multiply_sine_fusion
  2.7 105.3 %step.1 = (bf16[16,256,128]{2,1,0:T(8,128)(2,1)}, bf16[16,128,128]{2,1,0:T(8,128)(2,1)}) custom-call(bf16[256,768]{1,0:T(8,128)(2,1)} %refs_0_.1, bf16[256,512]{1,0:T(8,128)(2,1)} %refs_1_.1, bf16[64,256]{1,0:T(8,128)(2,1)} %bitcast.21, f32[32,256]{1,0:T(8,128)} %get-tuple-element.9.refs_3_, f32[32,256]{1,0:T(8,128)} %get-tuple-element.8.refs_4_, ...), custom_call_target="tpu_custom_call" | custom-call | tf_op jit(solution)/shard_map/step/pallas_call | solution.py:505
  108.0 1.5 %copy.19 = bf16[256,16,128]{0,2,1:T(8,128)(2,1)S(1)} copy(bf16[256,16,128]{2,0,1:T(8,128)(2,1)} %bitcast.15) | data formatting | bytes 2097152 | tf_op jit(solution)/shard_map/transpose | solution.py:519
  109.5 0.0 copy-start
  109.5 1.4 %copy.21 = bf16[256,2048]{1,0:T(8,128)(2,1)} copy(bf16[256,2048]{0,1:T(8,128)(2,1)S(1)} %bitcast.13) | data formatting | bytes 2097152
  111.0 0.0 copy-done
  111.0 0.3 copy.20
  111.3 1.0 copy.22
  (2 shorter events, 0.0 us)
Async XLA Ops:
  0.6 0.7 copy-start.1
  109.5 1.4 %copy-start = (bf16[16,128,128]{2,1,0:T(8,128)(2,1)S(1)}, bf16[16,128,128]{2,1,0:T(8,128)(2,1)}, u32[]{:S(2)}) copy-start(bf16[16,128,128]{2,1,0:T(8,128)(2,1)} %get-tuple-element.5) | copy-start | bytes 1572868

commit v2 on v1

--- a/solution.py
+++ b/solution.py
@@ -3,6 +3,7 @@
 
 import jax
 import jax.numpy as jnp
+import numpy as np
 from jax import lax
 from jax.experimental import pallas as pl
 from jax.experimental.pallas import tpu as pltpu
@@ -23,6 +24,7 @@
 EP = ("z", "x")
 TP = ("y", "c")
 NX = 4
+PARTS = 4
 
 
 def dot(a, b, on_a=1, on_b=0):
@@ -65,21 +67,25 @@
             wait()
 
 
-def ring_gather(send, axis, size, buf, slot, send_sem, recv_sem, pair=None):
+def cuts(rows, parts):
+    edges = [rows * i // parts // 16 * 16 for i in range(parts)] + [rows]
+    return [(lo, hi - lo) for lo, hi in zip(edges, edges[1:])]
+
+
+def ring_gather(send, axis, size, piece, rows, parts, send_sem, recv_sem, pair=None):
     me = lax.axis_index(axis)
     ways = ({axis: lax.rem(me + 1, size)}, {axis: lax.rem(me + size - 1, size)})
     steps = size // 2
-    rows = buf.shape[1] // 2
-
-    def part(offset, half):
-        return buf.at[slot(lax.rem(me + offset + size, size)), pl.ds(half * rows, rows)]
-
-    def in_use(step, way, half):
-        return step < steps or way == half
-
-    def hop(step, way, half):
-        ref = part((1 - step) if way == 0 else (step - 1), half)
-        at = (way, step - 1, half)
+
+    def part(offset, i):
+        return piece(lax.rem(me + offset + size, size), *cuts(rows, parts)[i])
+
+    def in_use(step, way, i):
+        return step < steps or way == 2 * i // parts
+
+    def hop(step, way, i):
+        ref = part((1 - step) if way == 0 else (step - 1), i)
+        at = (way, step - 1, i)
         return (ref, ref, send_sem.at[at], recv_sem.at[at], ways[way])
 
     def hand(ref, at):
@@ -87,109 +93,203 @@
             device, pair_send, pair_recv = pair
             send.start(ref, ref, pair_send.at[at], pair_recv.at[at], device)
 
-    for half in range(2):
-        for way in range(2):
-            if in_use(1, way, half):
-                send.start(*hop(1, way, half))
+    order = [(i + half * parts // 2, way) for i in range(parts // 2) for half in range(2) for way in range(2)]
+    for i, way in order:
+        if in_use(1, way, i):
+            send.start(*hop(1, way, i))
     if pair is not None:
-        for half in range(2):
-            hand(part(0, half), (0, steps, half))
+        for i in range(parts):
+            hand(part(0, i), (0, steps, i))
     yield
     for step in range(1, steps + 1):
-        for half in range(2):
-            for way in range(2):
-                if in_use(step, way, half):
-                    at = (way, step - 1, half)
-                    ref = part(-step if way == 0 else step, half)
-                    send.copy(ref, ref, send_sem.at[at], recv_sem.at[at], ways[way]).wait_recv()
-                    if step < steps and in_use(step + 1, way, half):
-                        send.start(*hop(step + 1, way, half))
-                    hand(ref, at)
-        yield
-
-
-def pair_arrived(send, size, axis, buf, slot, step, pair):
+        for i, way in order:
+            if in_use(step, way, i):
+                at = (way, step - 1, i)
+                ref = part(-step if way == 0 else step, i)
+                send.copy(ref, ref, send_sem.at[at], recv_sem.at[at], ways[way]).wait_recv()
+                if step < steps and in_use(step + 1, way, i):
+                    send.start(*hop(step + 1, way, i))
+                hand(ref, at)
+        yield
+
+
+def pair_arrived(send, size, axis, piece, rows, parts, step, pair):
     device, pair_send, pair_recv = pair
     me = lax.axis_index(axis)
     steps = size // 2
-    rows = buf.shape[1] // 2
     if step == 0:
-        todo = [((0, steps, half), 0, half) for half in range(2)]
+        todo = [((0, steps, i), 0, i) for i in range(parts)]
     else:
         todo = [
-            ((way, step - 1, half), -step if way == 0 else step, half)
-            for half in range(2) for way in range(2) if step < steps or way == half
+            ((way, step - 1, i), -step if way == 0 else step, i)
+            for i in range(parts) for way in range(2) if step < steps or way == 2 * i // parts
         ]
-    for at, offset, half in todo:
-        ref = buf.at[slot(lax.rem(me + offset + size, size)), pl.ds(half * rows, rows)]
+    for at, offset, i in todo:
+        ref = piece(lax.rem(me + offset + size, size), *cuts(rows, parts)[i])
         send.copy(ref, ref, pair_send.at[at], pair_recv.at[at], device).wait_recv()
 
 
-def product_scatter(send, size, product, part, given, ring, sems, pair_device, result):
-    pair_send, pair_recv, send_sem, recv_sem = sems
-    me, core = lax.axis_index("y"), lax.axis_index("c")
+def near_gather(send, piece, piece_other, rows, sems, device):
+    send_sem, recv_sem, pair_send, pair_recv = sems
+    size, half = 8, rows // 2
+    me = lax.axis_index("y")
+
+    def at_piece(offset):
+        return lax.rem(me + offset + size, size)
+
+    def span(k, way):
+        return (way * half, half) if k == 3 else (0, rows)
+
+    def copy(k, way, source, to):
+        ref = piece(at_piece(source), *span(k, way))
+        return (ref, ref, send_sem.at[way, k], recv_sem.at[way, k], {"y": at_piece(to)})
+
+    def hand(which, at, offset, lo, count):
+        ref = which(at_piece(offset), lo, count)
+        return (ref, ref, pair_send.at[at], pair_recv.at[at], device)
+
+    signs = (1, -1)
+    for k, distance in ((1, 2), (0, 1)):
+        for way, sign in enumerate(signs):
+            send.start(*copy(k, way, 0, sign * distance))
+    send.start(*hand(piece, (0, 4), 0, 0, rows))
+    yield
+    for k, distance in ((1, 2), (0, 1), (2, 3), (3, 4)):
+        for way, sign in enumerate(signs):
+            send.copy(*copy(k, way, -sign * distance, 0)).wait_recv()
+            if k == 1:
+                send.start(*copy(3, way, -sign * 2, sign * 2))
+                send.start(*copy(2, way, -sign * 2, sign))
+            send.start(*hand(piece, (way, k), -sign * distance, *span(k, way)))
+        if k != 1:
+            yield
+    send.copy(*hand(piece_other, (0, 4), 0, 0, rows)).wait_recv()
+    for k, distance in ((1, 2), (0, 1), (2, 3), (3, 4)):
+        for way, sign in enumerate(signs):
+            send.copy(*hand(piece_other, (way, k), -sign * distance, *span(k, way))).wait_recv()
+
+
+class PairSum:
+    def __init__(self, send, size, product, part, given, sems, device):
+        self.send, self.size, self.product, self.part, self.given = send, size, product, part, given
+        self.sems, self.device = sems, device
+        self.me, self.core = lax.axis_index("y"), lax.axis_index("c")
+        self.seen = set()
+
+    def at(self, offset):
+        return lax.rem(self.me + offset + self.size, self.size)
+
+    def copy(self, offset):
+        p, i = self.at(offset), offset % self.size
+        pair_send, pair_recv = self.sems
+        return (self.part.at[1 - self.core, p], self.given.at[p], pair_send.at[i], pair_recv.at[i], self.device)
+
+    def make(self, *offsets):
+        for offset in offsets:
+            p = self.at(offset)
+            both = self.product(p).astype(BF16)
+            self.part[0, p] = both[:, :LANES]
+            self.part[1, p] = both[:, LANES:]
+            self.send.start(*self.copy(offset))
+
+    def own(self, offset, where):
+        if offset % self.size not in self.seen:
+            self.seen.add(offset % self.size)
+            self.send.copy(*self.copy(offset)).wait_recv()
+        p = self.at(offset)
+        return self.part[self.core, p, where].astype(F32) + self.given[p, where].astype(F32)
+
+    def emit(self, offset, where, value, *to):
+        self.part[self.core, self.at(offset), where] = value.astype(BF16)
+        self.send.start(self.part.at[self.core, self.at(offset), where], *to)
+
+
+def ring_scatter(send, size, sums, ring, parts, sems, result):
+    send_sem, recv_sem = sems
+    me = lax.axis_index("y")
     ways = ({"y": lax.rem(me + 1, size)}, {"y": lax.rem(me + size - 1, size)})
     steps = size // 2
-    rows = part.shape[2] // 2
-    order = [steps]
-    for k in range(steps - 1, 0, -1):
-        order += [k, -k]
-    order += [0]
-    place = {offset % size: i for i, offset in enumerate(order)}
-    seen = set()
-
-    def at_piece(offset):
-        return lax.rem(me + offset + size, size)
-
-    def given_copy(offset):
-        p, i = at_piece(offset), place[offset % size]
-        return (part.at[1 - core, p], given.at[p], pair_send.at[i], pair_recv.at[i], pair_device)
-
-    for offset in order:
-        p = at_piece(offset)
-        both = product(p).astype(BF16)
-        part[0, p] = both[:, :LANES]
-        part[1, p] = both[:, LANES:]
-        send.start(*given_copy(offset))
-
-    def in_use(step, way, half):
-        return step >= 2 or way == half
-
-    def arrival(step, way, half):
-        at = (way, step - 1, half)
-        ref = ring.at[way, step - 1, pl.ds(half * rows, rows)]
+    spans = [pl.ds(*cut) for cut in cuts(ring.shape[2], parts)]
+
+    def in_use(step, way, i):
+        return step >= 2 or way == 2 * i // parts
+
+    def arrival(step, way, i):
+        at = (way, step - 1, i)
+        ref = ring.at[way, step - 1, spans[i]]
         send.copy(ref, ref, send_sem.at[at], recv_sem.at[at], ways[way]).wait_recv()
-        return ring[way, step - 1, pl.ds(half * rows, rows)].astype(F32)
-
-    def own(offset, half):
-        if offset % size not in seen:
-            seen.add(offset % size)
-            send.copy(*given_copy(offset)).wait_recv()
-        p, where = at_piece(offset), pl.ds(half * rows, rows)
-        return part[core, p, where].astype(F32) + given[p, where].astype(F32)
-
+        return ring[way, step - 1, spans[i]].astype(F32)
+
+    order = [(i + half * parts // 2, way) for i in range(parts // 2) for half in range(2) for way in range(2)]
+    sums.make(steps)
+    if steps > 1:
+        sums.make(steps - 1, 1 - steps)
+    for step in range(1, steps + 1):
+        for i, way in order:
+            if in_use(step, way, i):
+                offset = (steps - step + 1) * (1 if way == 0 else -1)
+                value = sums.own(offset, spans[i])
+                if step > 1 and in_use(step - 1, way, i):
+                    value = value + arrival(step - 1, way, i)
+                at = (way, step - 1, i)
+                sums.emit(
+                    offset, spans[i], value, ring.at[way, step - 1, spans[i]],
+                    send_sem.at[at], recv_sem.at[at], ways[way],
+                )
+        if steps - step > 1:
+            sums.make(steps - step - 1, 1 + step - steps)
+        elif steps - step == 1 or steps == 1:
+            sums.make(0)
+        yield
+    for i in range(parts):
+        value = sums.own(0, spans[i])
+        for way in range(2):
+            if in_use(steps, way, i):
+                value = value + arrival(steps, way, i)
+        result[spans[i]] = value.astype(BF16)
+
+
+def near_scatter(send, sums, held, sems, result):
+    send_sem, recv_sem = sems
+    rows = held.shape[2]
+    whole = pl.ds(0, rows)
+
+    def span(k, way):
+        return pl.ds(way * (rows // 2), rows // 2) if k == 1 else whole
+
+    def to(k, way, distance):
+        sign = 1 - 2 * way
+        return (
+            held.at[way, k, span(k, way)], send_sem.at[way, k], recv_sem.at[way, k],
+            {"y": sums.at(sign * distance)},
+        )
+
+    def arrival(k, way):
+        ref = held.at[way, k, span(k, way)]
+        send.copy(ref, *to(k, way, 1)).wait_recv()
+        return held[way, k, span(k, way)].astype(F32)
+
+    sums.make(4, 3, -3, 2, -2)
+    for way, sign in enumerate((1, -1)):
+        sums.emit(4 * sign, span(1, way), sums.own(4 * sign, span(1, way)), *to(1, way, 2))
+    for way, sign in enumerate((1, -1)):
+        sums.emit(3 * sign, whole, sums.own(3 * sign, whole), *to(0, way, 1))
+    sums.make(1, -1, 0)
     yield
-    for step in range(1, steps + 1):
-        for half in range(2):
-            for way in range(2):
-                if in_use(step, way, half):
-                    offset = (steps - step + 1) * (1 if way == 0 else -1)
-                    value = own(offset, half)
-                    if step > 1 and in_use(step - 1, way, half):
-                        value = value + arrival(step - 1, way, half)
-                    p, where, at = at_piece(offset), pl.ds(half * rows, rows), (way, step - 1, half)
-                    part[core, p, where] = value.astype(BF16)
-                    send.start(
-                        part.at[core, p, where], ring.at[way, step - 1, where],
-                        send_sem.at[at], recv_sem.at[at], ways[way],
-                    )
-        yield
-    for half in range(2):
-        value = own(0, half)
+    for way, sign in enumerate((1, -1)):
+        value = sums.own(2 * sign, whole) + arrival(0, way)
+        far = arrival(1, way)
+        pad = jnp.zeros_like(far)
+        value = value + jnp.concatenate([far, pad] if way == 0 else [pad, far], axis=0)
+        sums.emit(2 * sign, whole, value, *to(3, way, 2))
+    for way, sign in enumerate((1, -1)):
+        sums.emit(sign, whole, sums.own(sign, whole), *to(2, way, 1))
+    yield
+    value = sums.own(0, whole)
+    for k in (2, 3):
         for way in range(2):
-            if in_use(steps, way, half):
-                value = value + arrival(steps, way, half)
-        result[pl.ds(half * rows, rows)] = value.astype(BF16)
+            value = value + arrival(k, way)
+    result[...] = value.astype(BF16)
 
 
 def exchange(send, nz, nx, src, dst, send_sem, recv_sem):
@@ -227,7 +327,7 @@
 
 def kernel(sizes, *refs):
     nz, nx, ny, cap, spaced = sizes
-    (query_latent, shared_latent, rotary_key, cosine, sine, query_gain, shared_gain, plain_weight, turn_weight,
+    (query_latent, shared_latent, rotary_key, inside_cos, inside_sin, block_cos, block_sin, query_gain, shared_gain, plain_weight, turn_weight,
      key_weight, value_weight, mixer_weight, tokens, token_gain, routing, routing_weight, gate, up, down,
      mixer_out, expert_out, *scratch) = refs
     (out_rows, in_rows, pack, mix_high, mix_low, gath, gate_up, hidden, part_e, given_e, ring_e, back_out, back_in,
@@ -252,8 +352,24 @@
             barrier, inc=1, device_id={"z": to // nx, "x": lax.rem(to, nx)}, device_id_type=MESH
         )
 
-    for device in ({"y": lax.rem(y + 1, ny)}, {"y": lax.rem(y + ny - 1, ny)}, other):
+    greeted = [{"y": lax.rem(y + d + ny, ny)} for d in ((1, -1, 2, -2) if ny == 8 else (1, -1))] + [other]
+    for device in greeted:
         pl.semaphore_signal(barrier, inc=1, device_id=device, device_id_type=MESH)
+
+    def gather_columns(ref, sems):
+        def piece(p, lo, size):
+            return ref.at[pl.ds(lo, size), pl.ds(pl.multiple_of((2 * p + core) * LANES, LANES), LANES)]
+
+        def piece_other(p, lo, size):
+            return ref.at[pl.ds(lo, size), pl.ds(pl.multiple_of((2 * p + 1 - core) * LANES, LANES), LANES)]
+
+        if ny == 8:
+            yield from near_gather(send, piece, piece_other, ref.shape[0], sems, other)
+        else:
+            pair = (other, *sems[2:])
+            yield from ring_gather(send, "y", ny, piece, ref.shape[0], 2, *sems[:2], pair)
+            for step in range(ny // 2 + 1):
+                pair_arrived(send, ny, "y", piece_other, ref.shape[0], 2, step, pair)
 
     def expert_chain():
         width = pl.ds(pl.multiple_of(turn * LANES, LANES), LANES)
@@ -274,11 +390,13 @@
         ).astype(BF16)
         rank = dot(member, earlier).astype(BF16)
         slots = count * spaced
-        shift = spaced.bit_length() - 1
-        spread = jnp.where(
-            lax.shift_right_logical(iota((slots, count), 0), shift) == iota((slots, count), 1), 1.0, 0.0
-        ).astype(BF16)
-        place = (iota((slots, count_of), 0) & (spaced - 1)).astype(F32)
+
+        def block(line):
+            return ((line.astype(F32) + 0.5) * (1.0 / spaced)).astype(jnp.int32)
+
+        spread = jnp.where(block(iota((slots, count), 0)) == iota((slots, count), 1), 1.0, 0.0).astype(BF16)
+        line = iota((slots, count_of), 0)
+        place = (line - block(line) * spaced).astype(F32)
         chosen = (dot(spread, member) > 0.5) & (dot(spread, rank) == place)
         high = weight.astype(BF16)
         low = (weight - high.astype(F32)).astype(BF16)
@@ -289,15 +407,18 @@
         arrive = exchange(send, nz, nx, out_rows, in_rows, s_a, r_a)
         yield
         column = iota(pack.shape, 1)
-        inner = column & (spaced - 1)
-        goal = jnp.where(inner < cap, lax.shift_right_logical(column, shift) * cap + inner, -1)
+        inner = column - block(column) * spaced
+        goal = jnp.where(inner < cap, block(column) * cap + inner, -1)
         pack[...] = jnp.where(goal == iota(pack.shape, 0), 1.0, 0.0).astype(BF16)
         arrive()
         gath[turn] = dot(pack[...], in_rows[...].reshape(slots, LANES)).astype(BF16)
         slot = lambda p: 2 * p + core
         slot_other = lambda p: 2 * p + 1 - core
+        packed = gath.shape[1]
+        piece = lambda p, lo, size: gath.at[slot(p), pl.ds(lo, size)]
+        piece_other = lambda p, lo, size: gath.at[slot_other(p), pl.ds(lo, size)]
         pair = (other, sp_g, rp_g)
-        ring = ring_gather(send, "y", ny, gath, slot, s_g, r_g, pair)
+        ring = ring_gather(send, "y", ny, piece, packed, PARTS, s_g, r_g, pair)
         steps = ny // 2
         next(ring)
         gate_up[...] = jnp.zeros_like(gate_up)
@@ -315,11 +436,11 @@
         yield
         for step in range(1, steps + 1):
             next(ring)
-            pair_arrived(send, ny, "y", gath, slot_other, step - 1, pair)
+            pair_arrived(send, ny, "y", piece_other, packed, PARTS, step - 1, pair)
             consume_step(step - 1, slot_other)
             consume_step(step, slot)
             yield
-        pair_arrived(send, ny, "y", gath, slot_other, steps, pair)
+        pair_arrived(send, ny, "y", piece_other, packed, PARTS, steps, pair)
         consume_step(steps, slot_other)
         gate_pre = jnp.minimum(gate_up[:, :LANES], CLAMP_LIMIT)
         up_pre = jnp.clip(gate_up[:, LANES:], -CLAMP_LIMIT, CLAMP_LIMIT)
@@ -328,32 +449,33 @@
         def product(p):
             return dot(hidden[...], down[:, pl.ds(pl.multiple_of(2 * LANES * p, 2 * LANES), 2 * LANES)])
 
-        yield from product_scatter(
-            send, ny, product, part_e, given_e, ring_e, (sp_e, rp_e, s_e, r_e), other, result_e
-        )
+        sums = PairSum(send, ny, product, part_e, given_e, (sp_e, rp_e), other)
+        yield from ring_scatter(send, ny, sums, ring_e, PARTS, (s_e, r_e), result_e)
         back_out[...] = dot(pack[...], result_e[...], 0, 0).astype(BF16).reshape(back_out.shape)
         arrive = exchange(send, nz, nx, back_out, back_in, s_b, r_b)
         yield
         arrive()
         back = back_in[...].reshape(slots, LANES)
         mixed = dot(mix_high[...], back, 0, 0) + dot(mix_low[...], back, 0, 0)
-        expert_out[turn] = mixed.astype(BF16)
-        pair = (other, sp_f, rp_f)
-        yield from ring_gather(send, "y", ny, expert_out, slot, s_f, r_f, pair)
-        for step in range(steps + 1):
-            pair_arrived(send, ny, "y", expert_out, slot_other, step, pair)
+        expert_out[:, width] = mixed.astype(BF16)
+        yield from gather_columns(expert_out, (s_f, r_f, sp_f, rp_f))
 
     def mixer_chain():
         scale = (NOPE + ROPE) ** -0.5 * math.log2(math.e)
+        mine = iota(block_cos.shape, 1) == me
+        cos_b = jnp.sum(jnp.where(mine, block_cos[...], 0.0), axis=1, keepdims=True)
+        sin_b = jnp.sum(jnp.where(mine, block_sin[...], 0.0), axis=1, keepdims=True)
+        cosine = inside_cos[...] * cos_b - inside_sin[...] * sin_b
+        sine = inside_sin[...] * cos_b + inside_cos[...] * sin_b
         latent = normed(query_latent, query_gain)
         queries[x, :rows] = dot(latent, plain_weight[...]).astype(BF16)
-        raw = turned(dot(turn_weight[...], latent, 1, 1), cosine[...], sine[...])
+        raw = turned(dot(turn_weight[...], latent, 1, 1), cosine, sine)
         raw = jnp.concatenate([raw, jnp.zeros_like(raw)], axis=0)
         queries[x, rows:] = raw.T.astype(BF16)
         shared = normed(shared_latent, shared_gain)
         keys[z, :rows] = dot(shared, key_weight[...]).astype(BF16)
         keys[z, rows : 2 * rows] = dot(shared, value_weight[...]).astype(BF16)
-        raw = turned(rotary_key[...].astype(F32), cosine[...], sine[...])
+        raw = turned(rotary_key[...].astype(F32), cosine, sine)
         raw = jnp.concatenate([raw[:, : rows // 2], raw[:, rows // 2 :]], axis=0)
         keys[z, 2 * rows :] = raw.T.astype(BF16)
         yield
@@ -361,7 +483,9 @@
         from_x = [lax.rem(x + nx - d, nx) for d in range(nx)]
         for d in range(1, nx):
             send.start(queries.at[x], queries.at[x], s_q.at[d], r_q.at[d], {"x": to_x[d]})
-        ring = ring_gather(send, "z", nz, keys, lambda p: p, s_k, r_k)
+        ring = ring_gather(
+            send, "z", nz, lambda p, lo, size: keys.at[p, pl.ds(lo, size)], keys.shape[1], 2, s_k, r_k
+        )
         next(ring)
         yield
         for d in range(1, nx):
@@ -446,18 +570,18 @@
             columns = pl.ds(pl.multiple_of(2 * LANES * p, 2 * LANES), 2 * LANES)
             return dot(heads[...], mixer_weight[:, columns], 0, 0)
 
-        yield from product_scatter(
-            send, ny, product, part_m, given_m, ring_m, (sp_m, rp_m, s_m, r_m), other, mixer_out.at[turn]
-        )
-        pair = (other, sp_h, rp_h)
-        yield from ring_gather(send, "y", ny, mixer_out, lambda p: 2 * p + core, s_h, r_h, pair)
-        for step in range(ny // 2 + 1):
-            pair_arrived(send, ny, "y", mixer_out, lambda p: 2 * p + 1 - core, step, pair)
+        sums = PairSum(send, ny, product, part_m, given_m, (sp_m, rp_m), other)
+        result = mixer_out.at[:, pl.ds(pl.multiple_of(turn * LANES, LANES), LANES)]
+        if ny == 8:
+            yield from near_scatter(send, sums, ring_m, (s_m, r_m), result)
+        else:
+            yield from ring_scatter(send, ny, sums, ring_m, 2, (s_m, r_m), result)
+        yield from gather_columns(mixer_out, (s_h, r_h, sp_h, rp_h))
 
     chains = [expert_chain(), mixer_chain()]
     for chain in chains:
         next(chain)
-    pl.semaphore_wait(barrier, count + 2)
+    pl.semaphore_wait(barrier, count - 1 + len(greeted))
     while chains:
         for chain in list(chains):
             try:
@@ -471,15 +595,19 @@
                key_weight, value_weight, mixer_weight, tokens, token_gain, routing, routing_weight, gate, up, down):
     nz, nx, ny, cap, spaced = sizes
     rows = query_latent.shape[0]
-    position = (lax.axis_index(EP) * rows + jnp.arange(rows, dtype=jnp.int32)).astype(F32)
-    half = ROPE // 2
-    frequency = ROTARY_BASE ** (-2.0 * jnp.arange(half, dtype=F32) / ROPE)
-    angles = position[None, :] * frequency[:, None]
     count, pieces = nz * nx, 2 * ny
+    frequency = ROTARY_BASE ** (-2.0 * np.arange(ROPE // 2) / ROPE)
+    inside = frequency[:, None] * np.arange(rows)
+    blocks = frequency[:, None] * (np.arange(count) * rows)
+    tables = [jnp.asarray(f(a), F32) for a in (inside, blocks) for f in (np.cos, np.sin)]
     slots, packed = count * spaced, count * cap
     count_of = tokens.shape[0]
     vmem, dma = pltpu.VMEM, pltpu.SemaphoreType.DMA
-    hops, handed = dma((2, ny // 2, 2)), dma((2, ny // 2 + 1, 2))
+    hops, handed = dma((2, ny // 2, PARTS)), dma((2, ny // 2 + 1, PARTS))
+    if ny == 8:
+        hops_m, hops_h, handed_h = dma((2, 4)), dma((2, 4)), dma((2, 5))
+    else:
+        hops_m, hops_h, handed_h = hops, hops, handed
     scratch = [
         vmem((count, spaced, LANES), BF16), vmem((count, spaced, LANES), BF16), vmem((packed, slots), BF16),
         vmem((slots, count_of), BF16), vmem((slots, count_of), BF16), vmem((pieces, packed, LANES), BF16),
@@ -492,21 +620,21 @@
         vmem((nx, LANES, rows), BF16), vmem((nx, 8, rows), F32), vmem((LANES, rows), BF16),
         vmem((2, ny, rows, LANES), BF16), vmem((ny, rows, LANES), BF16), vmem((2, ny // 2, rows, LANES), BF16),
         dma((count,)), dma((count,)), hops, hops, handed, handed, dma((ny,)), dma((ny,)), hops, hops,
-        dma((count,)), dma((count,)), hops, hops, handed, handed,
+        dma((count,)), dma((count,)), hops_h, hops_h, handed_h, handed_h,
         dma((nx,)), dma((nx,)), dma((2, nz // 2, 2)), dma((2, nz // 2, 2)), dma((nx,)), dma((nx,)), dma((nx,)),
-        dma((nx,)), dma((ny,)), dma((ny,)), hops, hops, hops, hops, handed, handed,
+        dma((nx,)), dma((ny,)), dma((ny,)), hops_m, hops_m, hops_h, hops_h, handed_h, handed_h,
     ]
     spec = pl.BlockSpec(memory_space=pltpu.VMEM)
     operands = (
-        query_latent, shared_latent, rotary_key.T, jnp.cos(angles), jnp.sin(angles), query_gain[None],
+        query_latent, shared_latent, rotary_key.T, *tables, query_gain,
         shared_gain[None], plain_weight, turn_weight.T, key_weight, value_weight, mixer_weight, tokens,
         token_gain[None], routing.T, routing_weight.T, gate[0], up[0], down[0],
     )
-    mixer_out, expert_out = pl.pallas_call(
+    return pl.pallas_call(
         functools.partial(kernel, sizes),
         out_shape=(
-            jax.ShapeDtypeStruct((pieces, rows, LANES), BF16),
-            jax.ShapeDtypeStruct((pieces, count_of, LANES), BF16),
+            pltpu.VMEM((rows, pieces * LANES), BF16),
+            pltpu.VMEM((count_of, pieces * LANES), BF16),
         ),
         in_specs=[spec] * len(operands),
         out_specs=(spec, spec),
@@ -516,7 +644,6 @@
         ),
         name="step",
     )(*operands)
-    return tuple(a.transpose(1, 0, 2).reshape(a.shape[1], -1) for a in (mixer_out, expert_out))
 
 
 def build(mesh, nx, cap, spaced):
@@ -533,4 +660,4 @@
 
 
 def solution(mesh):
-    return build(mesh, NX, 21, 32)
+    return build(mesh, NX, 21, 24)

time: 112 us -> 102 us (0.911)
  Pallas kernels: 105 us -> 99.4 us
  local copies, waits for them, and re-layouts: 5.44 us -> 1.77 us
    pallas_call x1, Pallas kernels: 105 us -> 99.4 us  [per_device(): pl.pallas_call(functools.partial(kernel, sizes), out_shape=(pltpu.VMEM((r...]
    transpose x2 -> x0, local copies, waits for them, and re-layouts: 1.77 us -> none  [per_device(): a.transpose(1, 0, 2).reshape(a.shape[1], -1)]
    unnamed x6 -> x2, local copies, waits for them, and re-layouts: 3.09 us -> 1.77 us
where the time goes in v2:
time: 102 us
  Pallas kernels  99.4 us (97%)
  local copies, waits for them, and re-layouts  1.77 us (2%)
    pallas_call x1, Pallas kernels, per_device(): pl.pallas_call(functools.partial(kernel, sizes), out_shape=(pltpu.VMEM((r...  99.4 us

profile of v2, /device:TPU:1, one launch (start us, length us, event | category | flops | bytes accessed | tf_op | source)
XLA Modules:
  0.0 101.8 jit_solution(16328637994795370452)
XLA Ops:
  0.6 99.4 %step.1 = (bf16[256,2048]{1,0:T(8,128)(2,1)S(1)}, bf16[128,2048]{1,0:T(8,128)(2,1)S(1)}) custom-call(bf16[256,768]{1,0:T(8,128)(2,1)} %refs_0_.1, bf16[256,512]{1,0:T(8,128)(2,1)} %refs_1_.1, bf16[64,256]{1,0:T(8,128)(2,1)} %bitcast.13, f32[32,256]{1,0:T(8,128)} %constant.8.clone.refs_3_, f32[32,256]{1,0:T(8,128)} %constant.9.clone.refs_4_, ...), custom_call_target="tpu_custom_call" | custom-call | tf_op jit(solution)/shard_map/step/pallas_call | solution.py:633
  100.0 1.0 copy.25
  101.0 0.8 copy.26

commit v3 on v2

--- a/solution.py
+++ b/solution.py
@@ -25,6 +25,12 @@
 TP = ("y", "c")
 NX = 4
 PARTS = 4
+COUNT_IN = 21
+CLOCK = {
+    "start": 0.1, "arrive": 7.0, "gather": (9.5, 4.5, 3.8), "scatter": (27.0, 4.0, 4.0), "back": 53.0,
+    "last": 54.0, "keys": (1.0, 9.2, 6.3), "queries": 11.0, "attend": (11.5, 6.4), "merge": 33.5, "mixer": 34.0,
+    "mixer_gather": 48.0,
+}
 
 
 def dot(a, b, on_a=1, on_b=0):
@@ -72,16 +78,21 @@
     return [(lo, hi - lo) for lo, hi in zip(edges, edges[1:])]
 
 
-def ring_gather(send, axis, size, piece, rows, parts, send_sem, recv_sem, pair=None):
+def in_order(parts):
+    return [[(i + half * parts // 2, way) for half in range(2) for way in range(2)] for i in range(parts // 2)]
+
+
+def ring_gather(send, axis, size, piece, rows, parts, send_sem, recv_sem, clock, pair=None, far=True):
     me = lax.axis_index(axis)
     ways = ({axis: lax.rem(me + 1, size)}, {axis: lax.rem(me + size - 1, size)})
-    steps = size // 2
+    steps = size // 2 if far else size // 2 - 1
+    start, first, period = clock
 
     def part(offset, i):
         return piece(lax.rem(me + offset + size, size), *cuts(rows, parts)[i])
 
     def in_use(step, way, i):
-        return step < steps or way == 2 * i // parts
+        return step <= steps and (2 * step < size or way == 2 * i // parts)
 
     def hop(step, way, i):
         ref = part((1 - step) if way == 0 else (step - 1), i)
@@ -93,24 +104,24 @@
             device, pair_send, pair_recv = pair
             send.start(ref, ref, pair_send.at[at], pair_recv.at[at], device)
 
-    order = [(i + half * parts // 2, way) for i in range(parts // 2) for half in range(2) for way in range(2)]
-    for i, way in order:
-        if in_use(1, way, i):
-            send.start(*hop(1, way, i))
+    for group in in_order(parts):
+        for i, way in group:
+            if in_use(1, way, i):
+                send.start(*hop(1, way, i))
     if pair is not None:
         for i in range(parts):
-            hand(part(0, i), (0, steps, i))
-    yield
+            hand(part(0, i), (0, size // 2, i))
     for step in range(1, steps + 1):
-        for i, way in order:
-            if in_use(step, way, i):
-                at = (way, step - 1, i)
-                ref = part(-step if way == 0 else step, i)
-                send.copy(ref, ref, send_sem.at[at], recv_sem.at[at], ways[way]).wait_recv()
-                if step < steps and in_use(step + 1, way, i):
-                    send.start(*hop(step + 1, way, i))
-                hand(ref, at)
-        yield
+        for g, group in enumerate(in_order(parts)):
+            yield (step, start + first + period * (step - 1 + 2 * g / parts))
+            for i, way in group:
+                if in_use(step, way, i):
+                    at = (way, step - 1, i)
+                    ref = part(-step if way == 0 else step, i)
+                    send.copy(ref, ref, send_sem.at[at], recv_sem.at[at], ways[way]).wait_recv()
+                    if in_use(step + 1, way, i):
+                        send.start(*hop(step + 1, way, i))
+                    hand(ref, at)
 
 
 def pair_arrived(send, size, axis, piece, rows, parts, step, pair):
@@ -129,7 +140,7 @@
         send.copy(ref, ref, pair_send.at[at], pair_recv.at[at], device).wait_recv()
 
 
-def near_gather(send, piece, piece_other, rows, sems, device):
+def near_gather(send, piece, piece_other, rows, sems, device, start):
     send_sem, recv_sem, pair_send, pair_recv = sems
     size, half = 8, rows // 2
     me = lax.axis_index("y")
@@ -153,16 +164,15 @@
         for way, sign in enumerate(signs):
             send.start(*copy(k, way, 0, sign * distance))
     send.start(*hand(piece, (0, 4), 0, 0, rows))
-    yield
     for k, distance in ((1, 2), (0, 1), (2, 3), (3, 4)):
+        yield start + (4.0, 4.0, 7.0, 8.0)[distance - 1]
         for way, sign in enumerate(signs):
             send.copy(*copy(k, way, -sign * distance, 0)).wait_recv()
             if k == 1:
                 send.start(*copy(3, way, -sign * 2, sign * 2))
                 send.start(*copy(2, way, -sign * 2, sign))
             send.start(*hand(piece, (way, k), -sign * distance, *span(k, way)))
-        if k != 1:
-            yield
+    yield start + 9.0
     send.copy(*hand(piece_other, (0, 4), 0, 0, rows)).wait_recv()
     for k, distance in ((1, 2), (0, 1), (2, 3), (3, 4)):
         for way, sign in enumerate(signs):
@@ -204,7 +214,7 @@
         self.send.start(self.part.at[self.core, self.at(offset), where], *to)
 
 
-def ring_scatter(send, size, sums, ring, parts, sems, result):
+def ring_scatter(send, size, sums, ring, parts, sems, result, clock):
     send_sem, recv_sem = sems
     me = lax.axis_index("y")
     ways = ({"y": lax.rem(me + 1, size)}, {"y": lax.rem(me + size - 1, size)})
@@ -220,27 +230,29 @@
         send.copy(ref, ref, send_sem.at[at], recv_sem.at[at], ways[way]).wait_recv()
         return ring[way, step - 1, spans[i]].astype(F32)
 
-    order = [(i + half * parts // 2, way) for i in range(parts // 2) for half in range(2) for way in range(2)]
+    start, first, period = clock
     sums.make(steps)
     if steps > 1:
         sums.make(steps - 1, 1 - steps)
     for step in range(1, steps + 1):
-        for i, way in order:
-            if in_use(step, way, i):
-                offset = (steps - step + 1) * (1 if way == 0 else -1)
-                value = sums.own(offset, spans[i])
-                if step > 1 and in_use(step - 1, way, i):
-                    value = value + arrival(step - 1, way, i)
-                at = (way, step - 1, i)
-                sums.emit(
-                    offset, spans[i], value, ring.at[way, step - 1, spans[i]],
-                    send_sem.at[at], recv_sem.at[at], ways[way],
-                )
+        for g, group in enumerate(in_order(parts)):
+            yield start + (first + period * (step - 2 + 2 * g / parts) if step > 1 else 0.0)
+            for i, way in group:
+                if in_use(step, way, i):
+                    offset = (steps - step + 1) * (1 if way == 0 else -1)
+                    value = sums.own(offset, spans[i])
+                    if step > 1 and in_use(step - 1, way, i):
+                        value = value + arrival(step - 1, way, i)
+                    at = (way, step - 1, i)
+                    sums.emit(
+                        offset, spans[i], value, ring.at[way, step - 1, spans[i]],
+                        send_sem.at[at], recv_sem.at[at], ways[way],
+                    )
         if steps - step > 1:
             sums.make(steps - step - 1, 1 + step - steps)
         elif steps - step == 1 or steps == 1:
             sums.make(0)
-        yield
+    yield start + first + period * (steps - 0.5)
     for i in range(parts):
         value = sums.own(0, spans[i])
         for way in range(2):
@@ -249,7 +261,7 @@
         result[spans[i]] = value.astype(BF16)
 
 
-def near_scatter(send, sums, held, sems, result):
+def near_scatter(send, sums, held, sems, result, start):
     send_sem, recv_sem = sems
     rows = held.shape[2]
     whole = pl.ds(0, rows)
@@ -269,13 +281,15 @@
         send.copy(ref, *to(k, way, 1)).wait_recv()
         return held[way, k, span(k, way)].astype(F32)
 
-    sums.make(4, 3, -3, 2, -2)
+    sums.make(4, 3, -3)
+    yield start + 1.0
+    sums.make(2, -2, 1, -1, 0)
+    yield start + 2.0
     for way, sign in enumerate((1, -1)):
         sums.emit(4 * sign, span(1, way), sums.own(4 * sign, span(1, way)), *to(1, way, 2))
     for way, sign in enumerate((1, -1)):
         sums.emit(3 * sign, whole, sums.own(3 * sign, whole), *to(0, way, 1))
-    sums.make(1, -1, 0)
-    yield
+    yield start + 8.0
     for way, sign in enumerate((1, -1)):
         value = sums.own(2 * sign, whole) + arrival(0, way)
         far = arrival(1, way)
@@ -284,7 +298,7 @@
         sums.emit(2 * sign, whole, value, *to(3, way, 2))
     for way, sign in enumerate((1, -1)):
         sums.emit(sign, whole, sums.own(sign, whole), *to(2, way, 1))
-    yield
+    yield start + 14.0
     value = sums.own(0, whole)
     for k in (2, 3):
         for way in range(2):
@@ -327,13 +341,15 @@
 
 def kernel(sizes, *refs):
     nz, nx, ny, cap, spaced = sizes
-    (query_latent, shared_latent, rotary_key, inside_cos, inside_sin, block_cos, block_sin, query_gain, shared_gain, plain_weight, turn_weight,
-     key_weight, value_weight, mixer_weight, tokens, token_gain, routing, routing_weight, gate, up, down,
-     mixer_out, expert_out, *scratch) = refs
-    (out_rows, in_rows, pack, mix_high, mix_low, gath, gate_up, hidden, part_e, given_e, ring_e, back_out, back_in,
-     result_e, queries, query_1, query_2, keys, peak, total, accum, share_out, stat_out, share_in, stat_in,
-     heads, part_m, given_m, ring_m,
-     s_a, r_a, s_g, r_g, sp_g, rp_g, sp_e, rp_e, s_e, r_e, s_b, r_b, s_f, r_f, sp_f, rp_f,
+    given, (mixer_out, expert_out) = refs[:COUNT_IN], refs[COUNT_IN : COUNT_IN + 2]
+    inputs, scratch = refs[COUNT_IN + 2 : 2 * COUNT_IN + 2], refs[2 * COUNT_IN + 2 :]
+    (routing, routing_weight, tokens, token_gain, query_latent, shared_latent, rotary_key, inside_cos, inside_sin,
+     block_cos, block_sin, query_gain, shared_gain, plain_weight, turn_weight, key_weight, value_weight,
+     gate, up, down, mixer_weight) = inputs
+    (out_rows, in_rows, out_far, in_far, pack, mix_high, mix_low, gath, gate_up, hidden, part_e, given_e, ring_e,
+     back_out, back_in, result_e, queries, query_1, query_2, keys, peak, total, accum, share_out, stat_out, share_in,
+     stat_in, heads, part_m, given_m, ring_m,
+     s_in, s_a, r_a, s_x, r_x, sp_x, rp_x, s_g, r_g, sp_g, rp_g, sp_e, rp_e, s_e, r_e, s_b, r_b, s_f, r_f, sp_f, rp_f,
      s_q, r_q, s_k, r_k, s_o, r_o, s_t, r_t, sp_m, rp_m, s_m, r_m, s_h, r_h, sp_h, rp_h) = scratch
     z, x, y, core = (lax.axis_index(a) for a in ("z", "x", "y", "c"))
     count = nz * nx
@@ -356,7 +372,15 @@
     for device in greeted:
         pl.semaphore_signal(barrier, inc=1, device_id=device, device_id_type=MESH)
 
-    def gather_columns(ref, sems):
+    loads = [pltpu.make_async_copy(a, b, s_in.at[i]) for i, (a, b) in enumerate(zip(given, inputs))]
+    for load in loads:
+        load.start()
+
+    def loaded(first, last):
+        for load in loads[first:last]:
+            load.wait()
+
+    def gather_columns(ref, sems, start):
         def piece(p, lo, size):
             return ref.at[pl.ds(lo, size), pl.ds(pl.multiple_of((2 * p + core) * LANES, LANES), LANES)]
 
@@ -364,18 +388,24 @@
             return ref.at[pl.ds(lo, size), pl.ds(pl.multiple_of((2 * p + 1 - core) * LANES, LANES), LANES)]
 
         if ny == 8:
-            yield from near_gather(send, piece, piece_other, ref.shape[0], sems, other)
+            yield from near_gather(send, piece, piece_other, ref.shape[0], sems, other, start)
         else:
             pair = (other, *sems[2:])
-            yield from ring_gather(send, "y", ny, piece, ref.shape[0], 2, *sems[:2], pair)
+            for _, when in ring_gather(send, "y", ny, piece, ref.shape[0], 2, *sems[:2], (start, 4.0, 4.0), pair):
+                yield when
             for step in range(ny // 2 + 1):
                 pair_arrived(send, ny, "y", piece_other, ref.shape[0], 2, step, pair)
 
     def expert_chain():
         width = pl.ds(pl.multiple_of(turn * LANES, LANES), LANES)
+        far = lax.rem(y + ny // 2, ny)
+        far_width = pl.ds(pl.multiple_of((2 * far + core) * LANES, LANES), LANES)
+        loaded(0, 4)
         wide = tokens[...].astype(F32)
         factor = lax.rsqrt(jnp.mean(wide * wide, axis=-1, keepdims=True) + EPSILON)
-        own = (tokens[:, width].astype(F32) * factor * token_gain[:, width]).astype(BF16)
+        own, own_far = (
+            (tokens[:, w].astype(F32) * factor * token_gain[:, w]).astype(BF16) for w in (width, far_width)
+        )
         count_of = own.shape[0]
         named = iota((count, count_of), 0)
         member = jnp.zeros((count, count_of), F32)
@@ -402,14 +432,17 @@
         low = (weight - high.astype(F32)).astype(BF16)
         mix_high[...] = jnp.where(chosen, dot(spread, high), 0.0).astype(BF16)
         mix_low[...] = jnp.where(chosen, dot(spread, low), 0.0).astype(BF16)
-        out_rows[...] = dot(jnp.where(chosen, 1.0, 0.0).astype(BF16), own).astype(BF16).reshape(out_rows.shape)
-        yield
+        chosen = jnp.where(chosen, 1.0, 0.0).astype(BF16)
+        out_rows[...] = dot(chosen, own).astype(BF16).reshape(out_rows.shape)
+        out_far[...] = dot(chosen, own_far).astype(BF16).reshape(out_far.shape)
+        yield 0.0
         arrive = exchange(send, nz, nx, out_rows, in_rows, s_a, r_a)
-        yield
         column = iota(pack.shape, 1)
         inner = column - block(column) * spaced
         goal = jnp.where(inner < cap, block(column) * cap + inner, -1)
         pack[...] = jnp.where(goal == iota(pack.shape, 0), 1.0, 0.0).astype(BF16)
+        gate_up[...] = jnp.zeros_like(gate_up)
+        yield CLOCK["arrive"]
         arrive()
         gath[turn] = dot(pack[...], in_rows[...].reshape(slots, LANES)).astype(BF16)
         slot = lambda p: 2 * p + core
@@ -418,10 +451,9 @@
         piece = lambda p, lo, size: gath.at[slot(p), pl.ds(lo, size)]
         piece_other = lambda p, lo, size: gath.at[slot_other(p), pl.ds(lo, size)]
         pair = (other, sp_g, rp_g)
-        ring = ring_gather(send, "y", ny, piece, packed, PARTS, s_g, r_g, pair)
-        steps = ny // 2
-        next(ring)
-        gate_up[...] = jnp.zeros_like(gate_up)
+        ring = ring_gather(send, "y", ny, piece, packed, PARTS, s_g, r_g, CLOCK["gather"], pair, False)
+        ahead = next(ring, None)
+        arrive_far = exchange(send, nz, nx, out_far, in_far, s_x, r_x)
 
         def consume(piece):
             rows_of = pl.ds(pl.multiple_of(piece * LANES, LANES), LANES)
@@ -432,16 +464,32 @@
             for offset in sorted({-step % ny, step % ny}):
                 consume(which(lax.rem(y + offset, ny)))
 
+        far_slot, far_other = slot(far), slot_other(far)
+        far_copy = (gath.at[far_slot], gath.at[far_slot], sp_x, rp_x, other)
+        loaded(17, 19)
         consume_step(0, slot)
-        yield
-        for step in range(1, steps + 1):
-            next(ring)
-            pair_arrived(send, ny, "y", piece_other, packed, PARTS, step - 1, pair)
-            consume_step(step - 1, slot_other)
-            consume_step(step, slot)
-            yield
-        pair_arrived(send, ny, "y", piece_other, packed, PARTS, steps, pair)
-        consume_step(steps, slot_other)
+        for step in range(1, ny // 2 + 1):
+            behind = step - 1
+            while ahead is not None and ahead[0] == step:
+                yield ahead[1]
+                ahead = next(ring, None)
+                if behind is not None:
+                    pair_arrived(send, ny, "y", piece_other, packed, PARTS, behind, pair)
+                    consume_step(behind, slot_other)
+                    behind = None
+            if behind is not None:
+                pair_arrived(send, ny, "y", piece_other, packed, PARTS, behind, pair)
+                consume_step(behind, slot_other)
+            if step == max(1, ny // 2 - 2):
+                arrive_far()
+                gath[far_slot] = dot(pack[...], in_far[...].reshape(slots, LANES)).astype(BF16)
+                send.start(*far_copy)
+                consume(far_slot)
+            if step < ny // 2:
+                consume_step(step, slot)
+        ref = gath.at[far_other]
+        send.copy(ref, ref, sp_x, rp_x, other).wait_recv()
+        consume(far_other)
         gate_pre = jnp.minimum(gate_up[:, :LANES], CLAMP_LIMIT)
         up_pre = jnp.clip(gate_up[:, LANES:], -CLAMP_LIMIT, CLAMP_LIMIT)
         hidden[...] = ((up_pre + 1.0) * (gate_pre * jax.nn.sigmoid(SLOPE * gate_pre))).astype(BF16)
@@ -449,19 +497,21 @@
         def product(p):
             return dot(hidden[...], down[:, pl.ds(pl.multiple_of(2 * LANES * p, 2 * LANES), 2 * LANES)])
 
+        loaded(19, 20)
         sums = PairSum(send, ny, product, part_e, given_e, (sp_e, rp_e), other)
-        yield from ring_scatter(send, ny, sums, ring_e, PARTS, (s_e, r_e), result_e)
+        yield from ring_scatter(send, ny, sums, ring_e, PARTS, (s_e, r_e), result_e, CLOCK["scatter"])
         back_out[...] = dot(pack[...], result_e[...], 0, 0).astype(BF16).reshape(back_out.shape)
         arrive = exchange(send, nz, nx, back_out, back_in, s_b, r_b)
-        yield
+        yield CLOCK["back"]
         arrive()
         back = back_in[...].reshape(slots, LANES)
         mixed = dot(mix_high[...], back, 0, 0) + dot(mix_low[...], back, 0, 0)
         expert_out[:, width] = mixed.astype(BF16)
-        yield from gather_columns(expert_out, (s_f, r_f, sp_f, rp_f))
+        yield from gather_columns(expert_out, (s_f, r_f, sp_f, rp_f), CLOCK["last"])
 
     def mixer_chain():
         scale = (NOPE + ROPE) ** -0.5 * math.log2(math.e)
+        loaded(4, 17)
         mine = iota(block_cos.shape, 1) == me
         cos_b = jnp.sum(jnp.where(mine, block_cos[...], 0.0), axis=1, keepdims=True)
         sin_b = jnp.sum(jnp.where(mine, block_sin[...], 0.0), axis=1, keepdims=True)
@@ -478,16 +528,16 @@
         raw = turned(rotary_key[...].astype(F32), cosine, sine)
         raw = jnp.concatenate([raw[:, : rows // 2], raw[:, rows // 2 :]], axis=0)
         keys[z, 2 * rows :] = raw.T.astype(BF16)
-        yield
+        yield CLOCK["start"]
+        keys_here.append(ring_gather(
+            send, "z", nz, lambda p, lo, size: keys.at[p, pl.ds(lo, size)], keys.shape[1], 2, s_k, r_k, CLOCK["keys"]
+        ))
+        ahead.append(next(keys_here[0], None))
         to_x = [lax.rem(x + d, nx) for d in range(nx)]
         from_x = [lax.rem(x + nx - d, nx) for d in range(nx)]
         for d in range(1, nx):
             send.start(queries.at[x], queries.at[x], s_q.at[d], r_q.at[d], {"x": to_x[d]})
-        ring = ring_gather(
-            send, "z", nz, lambda p, lo, size: keys.at[p, pl.ds(lo, size)], keys.shape[1], 2, s_k, r_k
-        )
-        next(ring)
-        yield
+        yield CLOCK["queries"]
         for d in range(1, nx):
             ref = queries.at[from_x[d]]
             send.copy(ref, ref, s_q.at[d], r_q.at[d], {"x": to_x[d]}).wait_recv()
@@ -527,10 +577,11 @@
             peak[...] = highest
 
         attend(z, True)
-        yield
         steps = nz // 2
         for step in range(1, steps + 1):
-            next(ring)
+            yield CLOCK["attend"][0] + CLOCK["attend"][1] * (step - 1)
+            while ahead[0] is not None and ahead[0][0] == step:
+                ahead[0] = next(keys_here[0], None)
 
             @pl.when(z >= step)
             def _():
@@ -541,7 +592,6 @@
                 def _():
                     attend(lax.rem(z + step, nz), False)
 
-            yield
         share = (accum[...] / total[...]).astype(BF16)
         for j in range(nx):
             span = slice(j * rows, (j + 1) * rows)
@@ -554,7 +604,7 @@
             send.start(stat_out.at[to_x[d]], stat_in.at[x], s_t.at[d], r_t.at[d], device)
         share_in[x] = share_out[x]
         stat_in[x] = stat_out[x]
-        yield
+        yield CLOCK["merge"]
         for d in range(1, nx):
             device = {"x": to_x[d]}
             for ref, s, r in ((share_in, s_o, r_o), (stat_in, s_t, r_t)):
@@ -570,24 +620,33 @@
             columns = pl.ds(pl.multiple_of(2 * LANES * p, 2 * LANES), 2 * LANES)
             return dot(heads[...], mixer_weight[:, columns], 0, 0)
 
+        loaded(20, 21)
+        yield CLOCK["mixer"]
         sums = PairSum(send, ny, product, part_m, given_m, (sp_m, rp_m), other)
         result = mixer_out.at[:, pl.ds(pl.multiple_of(turn * LANES, LANES), LANES)]
         if ny == 8:
-            yield from near_scatter(send, sums, ring_m, (s_m, r_m), result)
+            yield from near_scatter(send, sums, ring_m, (s_m, r_m), result, CLOCK["mixer"])
         else:
-            yield from ring_scatter(send, ny, sums, ring_m, 2, (s_m, r_m), result)
-        yield from gather_columns(mixer_out, (s_h, r_h, sp_h, rp_h))
-
-    chains = [expert_chain(), mixer_chain()]
-    for chain in chains:
-        next(chain)
+            yield from ring_scatter(send, ny, sums, ring_m, 2, (s_m, r_m), result, (CLOCK["mixer"], 3.5, 3.5))
+        yield from gather_columns(mixer_out, (s_h, r_h, sp_h, rp_h), CLOCK["mixer_gather"])
+
+    keys_here, ahead = [], []
+
+    def keys_chain():
+        yield CLOCK["keys"][0] + CLOCK["keys"][1]
+        while ahead[0] is not None:
+            ahead[0] = next(keys_here[0], None)
+            if ahead[0] is not None:
+                yield ahead[0][1]
+
+    chains = [expert_chain(), keys_chain(), mixer_chain()]
+    waiting = [(next(chain), i) for i, chain in enumerate(chains)]
     pl.semaphore_wait(barrier, count - 1 + len(greeted))
-    while chains:
-        for chain in list(chains):
-            try:
-                next(chain)
-            except StopIteration:
-                chains.remove(chain)
+    while waiting:
+        _, i = waiting.pop(waiting.index(min(waiting)))
+        when = next(chains[i], None)
+        if when is not None:
+            waiting.append((when, i))
     send.finish()
 
 
@@ -609,6 +668,7 @@
     else:
         hops_m, hops_h, handed_h = hops, hops, handed
     scratch = [
+        vmem((count, spaced, LANES), BF16), vmem((count, spaced, LANES), BF16),
         vmem((count, spaced, LANES), BF16), vmem((count, spaced, LANES), BF16), vmem((packed, slots), BF16),
         vmem((slots, count_of), BF16), vmem((slots, count_of), BF16), vmem((pieces, packed, LANES), BF16),
         vmem((packed, 2 * LANES), F32), vmem((packed, LANES), BF16), vmem((2, ny, packed, LANES), BF16),
@@ -619,24 +679,26 @@
         vmem((LANES, nx * rows), F32), vmem((nx, LANES, rows), BF16), vmem((nx, 8, rows), F32),
         vmem((nx, LANES, rows), BF16), vmem((nx, 8, rows), F32), vmem((LANES, rows), BF16),
         vmem((2, ny, rows, LANES), BF16), vmem((ny, rows, LANES), BF16), vmem((2, ny // 2, rows, LANES), BF16),
-        dma((count,)), dma((count,)), hops, hops, handed, handed, dma((ny,)), dma((ny,)), hops, hops,
+        dma((COUNT_IN,)), dma((count,)), dma((count,)), dma((count,)), dma((count,)), dma, dma,
+        hops, hops, handed, handed, dma((ny,)), dma((ny,)), hops, hops,
         dma((count,)), dma((count,)), hops_h, hops_h, handed_h, handed_h,
         dma((nx,)), dma((nx,)), dma((2, nz // 2, 2)), dma((2, nz // 2, 2)), dma((nx,)), dma((nx,)), dma((nx,)),
         dma((nx,)), dma((ny,)), dma((ny,)), hops_m, hops_m, hops_h, hops_h, handed_h, handed_h,
     ]
     spec = pl.BlockSpec(memory_space=pltpu.VMEM)
     operands = (
-        query_latent, shared_latent, rotary_key.T, *tables, query_gain,
-        shared_gain[None], plain_weight, turn_weight.T, key_weight, value_weight, mixer_weight, tokens,
-        token_gain[None], routing.T, routing_weight.T, gate[0], up[0], down[0],
+        routing.T, routing_weight.T, tokens, token_gain[None], query_latent, shared_latent, rotary_key.T, *tables,
+        query_gain, shared_gain[None], plain_weight, turn_weight.T, key_weight, value_weight,
+        gate[0], up[0], down[0], mixer_weight,
     )
+    scratch = [vmem(a.shape, a.dtype) for a in operands] + scratch
     return pl.pallas_call(
         functools.partial(kernel, sizes),
         out_shape=(
             pltpu.VMEM((rows, pieces * LANES), BF16),
             pltpu.VMEM((count_of, pieces * LANES), BF16),
         ),
-        in_specs=[spec] * len(operands),
+        in_specs=[pl.BlockSpec(memory_space=pltpu.HBM)] * len(operands),
         out_specs=(spec, spec),
         scratch_shapes=scratch,
         compiler_params=pltpu.CompilerParams(

time: 102 us -> 93.5 us (0.917)
  Pallas kernels: 99.4 us -> 91 us
    pallas_call x1, Pallas kernels: 99.4 us -> 91 us  [per_device(): pl.pallas_call(functools.partial(kernel, sizes), out_shape=(pltpu.VMEM((r...]
where the time goes in v3:
time: 93.5 us; the launch traced here: 93.4 us
  Pallas kernels  91 us (97%)
  local copies, waits for them, and re-layouts  1.77 us (2%)
    pallas_call x1, Pallas kernels, per_device(): pl.pallas_call(functools.partial(kernel, sizes), out_shape=(pltpu.VMEM((r...  91 us

profile of v3, /device:TPU:1, one launch (start us, length us, event | category | flops | bytes accessed | tf_op | source)
XLA Modules:
  0.0 93.4 jit_solution(11426421382564251679)
XLA Ops:
  0.6 91.0 %step.1 = (bf16[256,2048]{1,0:T(8,128)(2,1)S(1)}, bf16[128,2048]{1,0:T(8,128)(2,1)S(1)}) custom-call(s32[4,128]{1,0:T(4,128)} %bitcast.15, f32[4,128]{1,0:T(4,128)} %bitcast.16, bf16[128,2048]{1,0:T(8,128)(2,1)} %refs_2_.1, f32[1,2048]{1,0:T(1,128)} %bitcast.14, bf16[256,768]{1,0:T(8,128)(2,1)} %refs_4_.1, bf16[256,512]{1,0:T(8,128)(2,1)} %refs_5_.1, ...), custom_call_target="tpu_custom_call" | custom-call | tf_op jit(solution)/shard_map/step/pallas_call | solution.py:695
  91.7 1.0 %copy.25 = bf16[256,2048]{1,0:T(8,128)(2,1)} copy(bf16[256,2048]{1,0:T(8,128)(2,1)S(1)} %get-tuple-element.2) | data formatting | bytes 2097152
  92.6 0.8 copy.26

commit v4 on v3

--- a/solution.py
+++ b/solution.py
@@ -27,9 +27,9 @@
 PARTS = 4
 COUNT_IN = 21
 CLOCK = {
-    "start": 0.1, "arrive": 7.0, "gather": (9.5, 4.5, 3.8), "scatter": (27.0, 4.0, 4.0), "back": 53.0,
-    "last": 54.0, "keys": (1.0, 9.2, 6.3), "queries": 11.0, "attend": (11.5, 6.4), "merge": 33.5, "mixer": 34.0,
-    "mixer_gather": 48.0,
+    "local": 0.05, "more": 0.2, "start": 0.1, "arrive": 7.0, "gather": (9.5, 4.5, 3.8), "scatter": (27.0, 4.0, 4.0), "back": 54.8,
+    "last": 55.5, "keys": (1.0, (10.2, 18.7, 22.9, 26.5), None), "queries": 11.0, "attend": (11.9, 18.9, 23.0, 29.0), "merge": 35.2, "mixer": 36.0, "mid": 44.0, "end": 50.0,
+    "mixer_gather": 50.5,
 }
 
 
@@ -68,8 +68,9 @@
         made.start()
         self.owed.append(made.wait_send)
 
-    def finish(self):
-        for wait in self.owed:
+    def finish(self, count=None):
+        now, self.owed = self.owed[:count], self.owed[len(self.owed[:count]) :]
+        for wait in now:
             wait()
 
 
@@ -113,7 +114,7 @@
             hand(part(0, i), (0, size // 2, i))
     for step in range(1, steps + 1):
         for g, group in enumerate(in_order(parts)):
-            yield (step, start + first + period * (step - 1 + 2 * g / parts))
+            yield (step, first[step - 1] if period is None else start + first + period * (step - 1 + 2 * g / parts))
             for i, way in group:
                 if in_use(step, way, i):
                     at = (way, step - 1, i)
@@ -289,7 +290,7 @@
         sums.emit(4 * sign, span(1, way), sums.own(4 * sign, span(1, way)), *to(1, way, 2))
     for way, sign in enumerate((1, -1)):
         sums.emit(3 * sign, whole, sums.own(3 * sign, whole), *to(0, way, 1))
-    yield start + 8.0
+    yield CLOCK["mid"]
     for way, sign in enumerate((1, -1)):
         value = sums.own(2 * sign, whole) + arrival(0, way)
         far = arrival(1, way)
@@ -298,7 +299,7 @@
         sums.emit(2 * sign, whole, value, *to(3, way, 2))
     for way, sign in enumerate((1, -1)):
         sums.emit(sign, whole, sums.own(sign, whole), *to(2, way, 1))
-    yield start + 14.0
+    yield CLOCK["end"]
     value = sums.own(0, whole)
     for k in (2, 3):
         for way in range(2):
@@ -428,15 +429,16 @@
         line = iota((slots, count_of), 0)
         place = (line - block(line) * spaced).astype(F32)
         chosen = (dot(spread, member) > 0.5) & (dot(spread, rank) == place)
+        member_row = jnp.where(chosen, 1.0, 0.0).astype(BF16)
+        out_rows[...] = dot(member_row, own).astype(BF16).reshape(out_rows.shape)
+        yield 0.0
+        arrive = exchange(send, nz, nx, out_rows, in_rows, s_a, r_a)
+        yield CLOCK["more"]
+        out_far[...] = dot(member_row, own_far).astype(BF16).reshape(out_far.shape)
         high = weight.astype(BF16)
         low = (weight - high.astype(F32)).astype(BF16)
         mix_high[...] = jnp.where(chosen, dot(spread, high), 0.0).astype(BF16)
         mix_low[...] = jnp.where(chosen, dot(spread, low), 0.0).astype(BF16)
-        chosen = jnp.where(chosen, 1.0, 0.0).astype(BF16)
-        out_rows[...] = dot(chosen, own).astype(BF16).reshape(out_rows.shape)
-        out_far[...] = dot(chosen, own_far).astype(BF16).reshape(out_far.shape)
-        yield 0.0
-        arrive = exchange(send, nz, nx, out_rows, in_rows, s_a, r_a)
         column = iota(pack.shape, 1)
         inner = column - block(column) * spaced
         goal = jnp.where(inner < cap, block(column) * cap + inner, -1)
@@ -455,14 +457,15 @@
         ahead = next(ring, None)
         arrive_far = exchange(send, nz, nx, out_far, in_far, s_x, r_x)
 
-        def consume(piece):
-            rows_of = pl.ds(pl.multiple_of(piece * LANES, LANES), LANES)
-            both = jnp.concatenate([gate[rows_of, :], up[rows_of, :]], axis=1)
-            gate_up[...] += dot(gath[piece], both)
+        def consume(*pieces):
+            lines = [pl.ds(pl.multiple_of(piece * LANES, LANES), LANES) for piece in pieces]
+            both = jnp.concatenate(
+                [jnp.concatenate([gate[at, :], up[at, :]], axis=1) for at in lines], axis=0
+            )
+            gate_up[...] += dot(jnp.concatenate([gath[piece] for piece in pieces], axis=1), both)
 
         def consume_step(step, which):
-            for offset in sorted({-step % ny, step % ny}):
-                consume(which(lax.rem(y + offset, ny)))
+            consume(*(which(lax.rem(y + offset, ny)) for offset in sorted({-step % ny, step % ny})))
 
         far_slot, far_other = slot(far), slot_other(far)
         far_copy = (gath.at[far_slot], gath.at[far_slot], sp_x, rp_x, other)
@@ -498,10 +501,12 @@
             return dot(hidden[...], down[:, pl.ds(pl.multiple_of(2 * LANES * p, 2 * LANES), 2 * LANES)])
 
         loaded(19, 20)
+        early = len(send.owed)
         sums = PairSum(send, ny, product, part_e, given_e, (sp_e, rp_e), other)
         yield from ring_scatter(send, ny, sums, ring_e, PARTS, (s_e, r_e), result_e, CLOCK["scatter"])
         back_out[...] = dot(pack[...], result_e[...], 0, 0).astype(BF16).reshape(back_out.shape)
         arrive = exchange(send, nz, nx, back_out, back_in, s_b, r_b)
+        send.finish(early)
         yield CLOCK["back"]
         arrive()
         back = back_in[...].reshape(slots, LANES)
@@ -510,6 +515,7 @@
         yield from gather_columns(expert_out, (s_f, r_f, sp_f, rp_f), CLOCK["last"])
 
     def mixer_chain():
+        yield CLOCK["local"]
         scale = (NOPE + ROPE) ** -0.5 * math.log2(math.e)
         loaded(4, 17)
         mine = iota(block_cos.shape, 1) == me
@@ -579,7 +585,7 @@
         attend(z, True)
         steps = nz // 2
         for step in range(1, steps + 1):
-            yield CLOCK["attend"][0] + CLOCK["attend"][1] * (step - 1)
+            yield CLOCK["attend"][step - 1]
             while ahead[0] is not None and ahead[0][0] == step:
                 ahead[0] = next(keys_here[0], None)
 
@@ -633,7 +639,7 @@
     keys_here, ahead = [], []
 
     def keys_chain():
-        yield CLOCK["keys"][0] + CLOCK["keys"][1]
+        yield CLOCK["keys"][1][0]
         while ahead[0] is not None:
             ahead[0] = next(keys_here[0], None)
             if ahead[0] is not None:

time: 93.5 us -> 92.6 us (level)
  Pallas kernels: 91 us -> 90 us
    pallas_call x1, Pallas kernels: 91 us -> 90 us  [per_device(): pl.pallas_call(functools.partial(kernel, sizes), out_shape=(pltpu.VMEM((r...]
where the time goes in v4:
time: 92.6 us; the launch traced here: 92.5 us
  Pallas kernels  90 us (97%)
  local copies, waits for them, and re-layouts  1.77 us (2%)
    pallas_call x1, Pallas kernels, per_device(): pl.pallas_call(functools.partial(kernel, sizes), out_shape=(pltpu.VMEM((r...  90 us

profile of v4, /device:TPU:1, one launch (start us, length us, event | category | flops | bytes accessed | tf_op | source)
XLA Modules:
  0.0 92.5 jit_solution(8407694430349755538)
XLA Ops:
  0.6 90.0 %step.1 = (bf16[256,2048]{1,0:T(8,128)(2,1)S(1)}, bf16[128,2048]{1,0:T(8,128)(2,1)S(1)}) custom-call(s32[4,128]{1,0:T(4,128)} %bitcast.15, f32[4,128]{1,0:T(4,128)} %bitcast.16, bf16[128,2048]{1,0:T(8,128)(2,1)} %refs_2_.1, f32[1,2048]{1,0:T(1,128)} %bitcast.14, bf16[256,768]{1,0:T(8,128)(2,1)} %refs_4_.1, bf16[256,512]{1,0:T(8,128)(2,1)} %refs_5_.1, ...), custom_call_target="tpu_custom_call" | custom-call | tf_op jit(solution)/shard_map/step/pallas_call | solution.py:701
  90.7 1.0 %copy.25 = bf16[256,2048]{1,0:T(8,128)(2,1)} copy(bf16[256,2048]{1,0:T(8,128)(2,1)S(1)} %get-tuple-element.2) | data formatting | bytes 2097152
  91.7 0.8 copy.26
